TPU v7x, 512 devices: a whole 4x4x16 slice. The times are simulated.
512 devices in a mesh: sp: 64 (over z, y), tp: 8 (over x, core).
Axes of the slice: x: 4, y: 4, z: 16, core: 2. Of those that a mesh axis runs over, the one named last changes fastest.
Arguments:
- tokens: bfloat16 [6144, 4, 1024], P(('sp', 'tp')), may hold values from -6 to 6
- in_gain: float32 [1024], replicated, may hold values from 0.1 to 1.9
- w_query: bfloat16 [1024, 1024], P('sp', 'tp'), may hold values from -0.1875 to 0.1875
- w_key: bfloat16 [1024, 1024], P('sp', 'tp'), may hold values from -0.1875 to 0.1875
- w_value: bfloat16 [1024, 1024], P('sp', 'tp'), may hold values from -0.1875 to 0.1875
- w_gate: bfloat16 [1024, 1024], P('sp', 'tp'), may hold values from -0.1875 to 0.1875
- w_beta: bfloat16 [1024, 8], P('sp', 'tp'), may hold values from -0.1875 to 0.1875
- conv_query: bfloat16 [4, 1024], P(None, 'tp'), may hold values from -3 to 3
- conv_key: bfloat16 [4, 1024], P(None, 'tp'), may hold values from -3 to 3
- conv_value: bfloat16 [4, 1024], P(None, 'tp'), may hold values from -3 to 3
- decay_rate: float32 [8], P('tp'), may hold values from 0.1 to 3
- out_gain: float32 [128], replicated, may hold values from 0.1 to 1.9
- w_out: bfloat16 [1024, 1024], P('tp', 'sp'), may hold values from -0.1875 to 0.1875
Outputs:
- mixed: bfloat16 [6144, 4, 1024], P(('sp', 'tp'))
All inputs are finite; a program needn't handle non-finite values.
Results may differ from a plain program's by a relative error of at most 0.02.
Values may be sent and summed in bfloat16 or wider, within the bound.
A program may use at most 64 MiB of HBM per device.

v0:
```python
import functools
import math

import jax
import jax.numpy as jnp
from jax import lax
from jax.experimental import pallas as pl
from jax.experimental.pallas import tpu as pltpu
from jax.sharding import PartitionSpec as P

PAD = 16
LANES = 128
epsilon = 1e-06
out_epsilon = 1e-10
f32 = jnp.float32
bf16 = jnp.bfloat16
NN, NT, TN = ((1,), (0,)), ((1,), (1,)), ((0,), (0,))


def dot(a, b, dims=NN):
    return lax.dot_general(
        a.astype(bf16), b.astype(bf16), (dims, ((), ())), preferred_element_type=f32
    )


def rms_scale(values_in, gain):
    values = values_in.astype(f32)
    scaled = values * lax.rsqrt(jnp.mean(values * values, axis=-1, keepdims=True) + epsilon)
    return (scaled * gain).astype(bf16)


def l2_normalize(array):
    return array * lax.rsqrt(jnp.sum(array * array, axis=-1, keepdims=True) + epsilon)


def unit_inverse(lower, row, col):
    size = lower.shape[0]
    near = ((row >> 1) == (col >> 1)) & (row != col)
    inverse = jnp.where(row == col, 1.0, 0.0) - jnp.where(near, lower, 0.0)
    level = 1
    while (1 << level) < size:
        mask = ((row >> (level + 1)) == (col >> (level + 1))) & ((row >> level) != (col >> level))
        cross = jnp.where(mask, lower, 0.0)
        inverse = inverse - dot(inverse, dot(cross, inverse))
        level += 1
    return inverse


def pair_terms(block, beta, taps, rate, depth):
    width = taps[0].shape[0]
    size = beta.shape[0]

    def conv(part):
        x = block[part].astype(f32)
        total = x * taps[part][width - 1 : width]
        for back in range(1, width):
            total = total + pltpu.roll(x, back, 0) * taps[part][width - 1 - back : width - back]
        total = total[PAD:]
        return total * jax.nn.sigmoid(total)

    query = l2_normalize(conv(0)) * depth ** (-0.5)
    keys = l2_normalize(conv(1))
    values = conv(2)
    row = lax.broadcasted_iota(jnp.int32, (size, size), 0)
    col = lax.broadcasted_iota(jnp.int32, (size, size), 1)
    decay = jnp.exp(-rate * jnp.maximum(row - col, 0).astype(f32))
    step = lax.broadcasted_iota(jnp.int32, (size, 1), 0).astype(f32)
    kept = jnp.exp(-rate * (step + 1.0))
    rest = jnp.exp(-rate * (size - 1.0 - step))
    weighted = keys * beta
    products = dot(jnp.concatenate([weighted, query], axis=0), keys, NT)
    lower = jnp.where(row > col, products[:size] * decay, 0.0)
    scores = jnp.where(row >= col, products[size:] * decay, 0.0)
    inverse = unit_inverse(lower, row, col)
    both = dot(inverse, jnp.concatenate([values * beta, weighted * kept], axis=1))
    seen = dot(scores, both)
    moved = dot(keys * rest, both, TN)
    return moved, query * kept - seen[:, depth:], seen[:, :depth]


def terms_kernel(heads, depth, shift, pre_ref, taps_ref, rate_ref, map_ref, read_ref, local_ref):
    head_width = heads * depth
    beta = jax.nn.sigmoid(pre_ref[0, PAD:, 4 * head_width :].astype(f32) + shift)
    for head in range(heads):
        places = [pl.ds(part * head_width + head * depth, depth) for part in range(3)]
        moved, read, local = pair_terms(
            [pre_ref[0, :, place] for place in places],
            beta[:, head : head + 1],
            [taps_ref[:, place] for place in places],
            rate_ref[head],
            depth,
        )
        map_ref[0, head] = moved.astype(bf16)
        read_ref[0, head] = read.astype(bf16)
        local_ref[0, head] = local


def chain_kernel(depth, kept_ref, map_ref, state_ref):
    state = jnp.zeros((depth, depth), f32)
    for index in range(map_ref.shape[0]):
        state_ref[index] = state.astype(bf16)
        state = (
            state * kept_ref[0]
            + map_ref[index, :, :depth].astype(f32)
            - dot(map_ref[index, :, depth:], state)
        )


def finish_kernel(heads, depth, read_ref, local_ref, state_ref, pre_ref, gain_ref, gated_ref):
    for head in range(heads):
        out = local_ref[0, head] + dot(read_ref[0, head], state_ref[0, head])
        out = out * lax.rsqrt(jnp.mean(out * out, axis=-1, keepdims=True) + out_epsilon)
        place = pl.ds(head * depth, depth)
        gate = pre_ref[0, PAD:, place].astype(f32)
        gate = gate * jax.nn.sigmoid(gate)
        gated_ref[0, :, place] = (out * gain_ref[...] * gate).astype(bf16)


def incoming_states(maps, kept):
    pairs, depth, _ = maps.shape
    length, here = lax.axis_size("sp"), lax.axis_index("sp")
    if pairs == length:
        mine = lax.all_to_all(maps, "sp", 0, 0, tiled=True)
        states = pl.pallas_call(
            functools.partial(chain_kernel, depth),
            out_shape=jax.ShapeDtypeStruct((length, depth, depth), bf16),
            in_specs=[
                pl.BlockSpec(memory_space=pltpu.SMEM),
                pl.BlockSpec(memory_space=pltpu.VMEM),
            ],
            out_specs=pl.BlockSpec(memory_space=pltpu.VMEM),
        )(lax.dynamic_slice_in_dim(kept, here, 1, 0), mine)
        return lax.all_to_all(states, "sp", 0, 0, tiled=True)
    everything = lax.all_gather(maps, "sp")

    def hop(index, state):
        moved = everything[index].astype(f32)
        erased = jnp.einsum(
            "pde,pev->pdv",
            moved[:, :, depth:].astype(bf16),
            state.astype(bf16),
            preferred_element_type=f32,
        )
        new = state * kept[:, None, None] + moved[:, :, :depth] - erased
        return jnp.where(index < here, new, state)

    state = lax.fori_loop(0, length, hop, jnp.zeros((pairs, depth, depth), f32))
    return state.astype(bf16)


def body(
    tokens,
    in_gain,
    w_query,
    w_key,
    w_value,
    w_gate,
    w_beta,
    conv_query,
    conv_key,
    conv_value,
    decay_rate,
    out_gain,
    w_out,
):
    seqs, width = tokens.shape[1], tokens.shape[2]
    head_width = w_query.shape[1]
    heads = w_beta.shape[1]
    depth = head_width // heads
    taps = conv_query.shape[0]
    length = lax.axis_size("sp")

    beta_pad = jnp.pad(w_beta, ((0, 0), (0, LANES - heads)))
    packed = jnp.concatenate([w_query, w_key, w_value, w_gate, beta_pad], axis=1)
    weights = lax.all_gather(packed, "sp", axis=0, tiled=True)
    full_out = lax.all_gather(w_out.T, "sp", axis=0, tiled=True)

    normed = jnp.swapaxes(rms_scale(tokens, in_gain), 0, 1)
    normed = lax.all_gather(normed, "tp", axis=1, tiled=True)
    span = normed.shape[1]
    history = lax.ppermute(
        normed[:, span - taps + 1 :], "sp", [(i, i + 1) for i in range(length - 1)]
    )
    filler = jnp.zeros((seqs, PAD - taps + 1, width), bf16)
    extended = jnp.concatenate([filler, history, normed], axis=1)
    rows = PAD + span
    pre = jnp.dot(
        extended.reshape(-1, width), weights, preferred_element_type=f32
    ).astype(bf16)
    pre = pre.reshape(seqs, rows, -1)

    total_tokens = span * length
    rate = decay_rate / total_tokens
    shift = math.log(depth / (4.0 * total_tokens))
    conv_taps = jnp.concatenate([conv_query, conv_key, conv_value], axis=1).astype(f32)

    def per_seq(*shape):
        return pl.BlockSpec((1,) + shape, lambda s: (s,) + (0,) * len(shape))

    maps, reads, locals_ = pl.pallas_call(
        functools.partial(terms_kernel, heads, depth, shift),
        grid=(seqs,),
        in_specs=[
            per_seq(rows, pre.shape[2]),
            pl.BlockSpec(conv_taps.shape, lambda s: (0, 0)),
            pl.BlockSpec(memory_space=pltpu.SMEM),
        ],
        out_specs=[
            per_seq(heads, depth, 2 * depth),
            per_seq(heads, span, depth),
            per_seq(heads, span, depth),
        ],
        out_shape=[
            jax.ShapeDtypeStruct((seqs, heads, depth, 2 * depth), bf16),
            jax.ShapeDtypeStruct((seqs, heads, span, depth), bf16),
            jax.ShapeDtypeStruct((seqs, heads, span, depth), f32),
        ],
    )(pre, conv_taps, rate)

    kept = jnp.tile(jnp.exp(-rate * span), seqs)
    states = incoming_states(maps.reshape(seqs * heads, depth, 2 * depth), kept)
    gated = pl.pallas_call(
        functools.partial(finish_kernel, heads, depth),
        grid=(seqs,),
        in_specs=[
            per_seq(heads, span, depth),
            per_seq(heads, span, depth),
            per_seq(heads, depth, depth),
            pl.BlockSpec((1, rows, head_width), lambda s: (s, 0, 3)),
            pl.BlockSpec((1, depth), lambda s: (0, 0)),
        ],
        out_specs=per_seq(span, head_width),
        out_shape=jax.ShapeDtypeStruct((seqs, span, head_width), bf16),
    )(reads, locals_, states.reshape(seqs, heads, depth, depth), pre, out_gain[None])

    mixed = lax.dot_general(
        gated, full_out, (((2,), (1,)), ((), ())), preferred_element_type=f32
    ).astype(bf16)
    mixed = lax.psum_scatter(mixed, "tp", scatter_dimension=1, tiled=True)
    return jnp.swapaxes(mixed, 0, 1)


def solution(mesh):
    placed = (
        P(("sp", "tp"), None, None),
        P(),
        P("sp", "tp"),
        P("sp", "tp"),
        P("sp", "tp"),
        P("sp", "tp"),
        P("sp", "tp"),
        P(None, "tp"),
        P(None, "tp"),
        P(None, "tp"),
        P("tp"),
        P(),
        P("tp", "sp"),
    )
    return jax.shard_map(
        body, mesh=mesh, in_specs=placed, out_specs=P(("sp", "tp"), None, None), check_vma=False
    )
```

profile of v0, /device:TPU:1, one launch (start us, length us, event | category | flops | bytes accessed | tf_op | source)
XLA Modules:
  0.0 523.6 jit_solution(4969400819812219106)
XLA Ops:
  10.8 1.0 fusion.8
  11.8 1.0 fusion.11
  12.8 20.1 %all_gather.12 = bf16[4,96,1024]{2,0,1:T(4,128)(2,1)S(1)} all-gather(bf16[4,12,1024]{2,0,1:T(4,128)(2,1)S(1)} %fusion.11), channel_id=1, replica_groups=mesh['sp'=64,'tp'=8] {'tp'}, dimensions={1}, use_global_device_ids=true | all-gather | bytes 884736 | tf_op jit(solution)/shard_map/all_gather | solution.py:179
  33.2 1.3 collective-permute-start
  36.1 109.6 %all-gather.4.cloned.1.call-done = bf16[1024,640]{1,0:T(8,128)(2,1)} async-done(((bf16[16,640]{1,0:T(8,128)(2,1)}), bf16[1024,640]{1,0:T(8,128)(2,1)}) %all-gather.4.cloned.1.call-update) | async-done | bytes 1310736 | tf_op jit(solution)/shard_map/all_gather | solution.py:175
  145.7 3.0 convolution_convert_fusion.1
  148.8 10.2 %shard_map.127 = (bf16[4,1,128,256]{3,2,1,0:T(8,128)(2,1)}, bf16[4,1,96,128]{3,2,1,0:T(8,128)(2,1)}, f32[4,1,96,128]{3,2,1,0:T(8,128)}) custom-call(bf16[4,112,640]{2,1,0:T(8,128)(2,1)} %bitcast.23, f32[4,384]{1,0:T(4,128)} %maximum_convert_fusion.taps_ref, f32[1]{0:T(128)S(6)} %div.11.rate_ref), custom_call_target="tpu_custom_call" | custom-call | tf_op jit(solution)/shard_map/pallas_call | solution.py:200
  159.1 76.3 %all_gather.15 = bf16[1024,128]{1,0:T(8,128)(2,1)S(1)} all-gather(bf16[16,128]{1,0:T(8,128)(2,1)S(1)} %bitcast.27), channel_id=1, replica_groups=mesh['sp'=64,'tp'=8] {'sp'}, dimensions={0}, use_global_device_ids=true | all-gather | bytes 266240 | tf_op jit(solution)/shard_map/all_gather | solution.py:176
  235.4 122.5 %all-gather.6.cloned.1.call-done = bf16[256,1,128,256]{3,2,1,0:T(8,128)(2,1)} async-done(((bf16[4,1,128,256]{3,2,1,0:T(8,128)(2,1)}), bf16[256,1,128,256]{3,2,1,0:T(8,128)(2,1)}) %all-gather.6.cloned.1.call-update) | async-done | bytes 16777232 | tf_op jit(solution)/shard_map/all_gather | solution.py:134
  358.0 77.6 %while.14 = (s32[]{:T(128)}, f32[4,128,128]{2,1,0:T(8,128)S(1)}, s32[]{:T(128)}, bf16[64,4,128,256]{3,2,1,0:T(8,128)(2,1)}, f32[]{:T(128)}, /*index=5*/s32[]{:T(128)}, s32[]{:T(128)}) while((s32[]{:T(128)}, f32[4,128,128]{2,1,0:T(8,128)S(1)}, s32[]{:T(128)}, bf16[64,4,128,256]{3,2,1,0:T(8,128)(2,1)}, f32[]{:T(128)}, ...), condition=%wide.region_2.3_spmd.clone, body=%wide.region_1.2_spmd.clone.sunk | while | flops 17301508 | bytes 2098799 | solution.py:147
  358.0 1.0 dynamic-slice_bitcast_fusion.3
  359.2 1.0 dynamic-slice_bitcast_fusion.3
  361.6 1.0 dynamic-slice_bitcast_fusion.3
  364.1 1.0 dynamic-slice_bitcast_fusion.3
  367.7 1.0 dynamic-slice_bitcast_fusion.3
  370.1 1.0 dynamic-slice_bitcast_fusion.3
  372.6 1.0 dynamic-slice_bitcast_fusion.3
  373.8 1.0 dynamic-slice_bitcast_fusion.3
  376.2 1.0 dynamic-slice_bitcast_fusion.3
  378.6 1.0 dynamic-slice_bitcast_fusion.3
  381.1 1.0 dynamic-slice_bitcast_fusion.3
  382.3 1.0 dynamic-slice_bitcast_fusion.3
  384.7 1.0 dynamic-slice_bitcast_fusion.3
  387.1 1.0 dynamic-slice_bitcast_fusion.3
  390.8 1.0 dynamic-slice_bitcast_fusion.3
  393.2 1.0 dynamic-slice_bitcast_fusion.3
  436.3 3.3 shard_map.128
  439.6 1.3 convolution_convert_fusion
  440.8 1.5 copy.28
  442.4 1.3 dynamic-slice
  444.3 71.2 %all-reduce.4.cloned.1.call-done = bf16[4,96,1024]{2,0,1:T(4,128)(2,1)} async-done(((bf16[4,96,1024]{2,0,1:T(4,128)(2,1)}), bf16[4,96,1024]{2,0,1:T(4,128)(2,1)}) %all-reduce.4.cloned.1.call-update) | async-done | bytes 786448
  515.5 1.6 dynamic-slice_bitcast_fusion.1
  (208 shorter events, 65.4 us)
Async XLA Ops:
  6.5 27.9 %copy-start.2 = (bf16[4,128]{1,0:T(4,128)(2,1)S(1)}, bf16[4,128]{1,0:T(4,128)(2,1)}, u32[]{:S(2)}) copy-start(bf16[4,128]{1,0:T(4,128)(2,1)} %param.24) | copy-start | bytes 3076
  6.5 27.9 %copy-start.3 = (bf16[4,128]{1,0:T(4,128)(2,1)S(1)}, bf16[4,128]{1,0:T(4,128)(2,1)}, u32[]{:S(2)}) copy-start(bf16[4,128]{1,0:T(4,128)(2,1)} %param.23) | copy-start | bytes 3076
  6.5 28.0 %copy-start.4 = (bf16[4,128]{1,0:T(4,128)(2,1)S(1)}, bf16[4,128]{1,0:T(4,128)(2,1)}, u32[]{:S(2)}) copy-start(bf16[4,128]{1,0:T(4,128)(2,1)} %param.22) | copy-start | bytes 3076
  6.5 139.2 %all-gather.4.cloned.1.call-start = ((), (), s32[]{:S(2)}) async-start(), calls=%async_computation | async-start | bytes 1331200 | tf_op jit(solution)/shard_map/all_gather | solution.py:175
  10.1 0.6 copy-start
  10.7 347.2 %all-gather.6.cloned.1.call-start = ((), (), s32[]{:S(2)}) async-start(), calls=%async_computation.1 | async-start | bytes 17039360 | tf_op jit(solution)/shard_map/all_gather | solution.py:134
  33.2 2.6 collective-permute-start
  145.7 13.4 %copy-start.1 = (bf16[128,16]{0,1:T(8,128)(2,1)S(1)}, bf16[128,16]{0,1:T(8,128)(2,1)}, u32[]{:S(2)}) copy-start(bf16[128,16]{0,1:T(8,128)(2,1)} %param.27) | copy-start | bytes 12292
  159.0 356.5 %all-reduce.4.cloned.1.call-start = ((), (), s32[]{:S(2)}) async-start(), calls=%async_computation.2 | async-start | bytes 1572864
Sparse Core Ops, SparseCore 0:
  10.9 134.8 all-gather.3
  159.1 198.8 all-gather.5
  442.5 72.9 all-reduce.3
where the time goes:
time: 527 us; the launch traced here: 524 us
  waiting for transfers between devices  303 us (57%)
  blocking collectives  96.4 us (18%)
  local copies, waits for them, and re-layouts  72.4 us (14%)
  matrix products  15.5 us (3%)
  between operations  14.6 us (3%)
  Pallas kernels  13.5 us (3%)
    all_gather x1, waiting for transfers between devices, incoming_states(): everything = lax.all_gather(maps, 'sp')  123 us
    all_gather x1, waiting for transfers between devices, body(): weights = lax.all_gather(packed, 'sp', axis=0, tiled=True)  110 us
    all_gather x1, blocking collectives, body(): full_out = lax.all_gather(w_out.T, 'sp', axis=0, tiled=True)  76.3 us
    unnamed x4, waiting for transfers between devices  71.3 us
    convert_element_type x64, local copies, waits for them, and re-layouts, hop(): moved = everything[index].astype(f32)  62.3 us
    all_gather x1, blocking collectives, body(): normed = lax.all_gather(normed, 'tp', axis=1, tiled=True)  20.1 us
    dot_general x64, matrix products, hop(): jnp.einsum('pde,pev->pdv', moved[:, :, depth:].astype(bf16), state.astype...  11.3 us
  transfers between devices with their start and end apart: 4, of which 3 were waited for; matrix products, arithmetic and copies ran while one was open for 1% of the time, Pallas kernels for 0%

commit v1 on v0

v1 whole, which is shorter than its diff:
```python
import functools
import math

import jax
import jax.numpy as jnp
from jax import lax
from jax.experimental import pallas as pl
from jax.experimental.pallas import tpu as pltpu
from jax.sharding import PartitionSpec as P

MESH = pl.DeviceIdType.MESH
PAD = 16
CHUNKS = 3
epsilon = 1e-06
out_epsilon = 1e-10
f32 = jnp.float32
bf16 = jnp.bfloat16
NN, NT, TN = ((1,), (0,)), ((1,), (1,)), ((0,), (0,))


def dot(a, b, dims=NN):
    return lax.dot_general(
        a.astype(bf16), b.astype(bf16), (dims, ((), ())), preferred_element_type=f32
    )


def iota(shape, axis):
    return lax.broadcasted_iota(jnp.int32, shape, axis)


def l2_normalize(array):
    return array * lax.rsqrt(jnp.sum(array * array, axis=-1, keepdims=True) + epsilon)


def unit_inverses(lowers, row, col):
    size = row.shape[0]
    near = ((row >> 1) == (col >> 1)) & (row != col)
    eye = jnp.where(row == col, 1.0, 0.0)
    inverses = [eye - jnp.where(near, lower, 0.0) for lower in lowers]
    level = 1
    while (1 << level) < size:
        mask = ((row >> (level + 1)) == (col >> (level + 1))) & ((row >> level) != (col >> level))
        inner = [dot(jnp.where(mask, l, 0.0), v) for l, v in zip(lowers, inverses)]
        inverses = [v - dot(v, w) for v, w in zip(inverses, inner)]
        level += 1
    return inverses


def compose(first, kept_first, second, kept_second):
    depth = first[0].shape[0]
    cross = dot(second[1], jnp.concatenate(first, axis=1))
    value = kept_second * first[0] + second[0] - cross[:, :depth]
    erase = kept_second * first[1] + kept_first * second[1] - cross[:, depth:]
    return value, erase


def mixer_kernel(
    sizes,
    tokens_ref,
    in_gain_ref,
    wq_ref,
    wk_ref,
    wv_ref,
    wg_ref,
    wb_ref,
    taps_ref,
    rate_ref,
    out_gain_ref,
    wo_ref,
    out_ref,
    weights,
    spread,
    strips,
    rows_buf,
    conv_buf,
    maps,
    parts,
    landed,
    w_send_y,
    w_send_z,
    w_recv,
    a_send,
    a_recv,
    b_send,
    b_recv,
    h_send,
    h_recv,
    m_send,
    m_recv,
    o_send,
    o_recv,
):
    depth, seqs, group, hops, here_rows, width = sizes
    total_tokens = hops * seqs * group * here_rows
    strip = seqs * here_rows
    span = group * strip
    size = span // CHUNKS
    sp, tp = lax.axis_index("sp"), lax.axis_index("tp")
    z, y = sp // seqs, sp % seqs
    up, down = (z + 1) % hops, (z + hops - 1) % hops

    def at(zz, yy, tt):
        return {"sp": zz * seqs + yy, "tp": tt}

    def copy(src, dst, send, recv, device):
        return pltpu.make_async_remote_copy(
            src_ref=src,
            dst_ref=dst,
            send_sem=send,
            recv_sem=recv,
            device_id=device,
            device_id_type=MESH,
        )

    me = at(z, y, tp)
    neighbours = [at(up, y, tp), at(down, y, tp)]
    far = [hops // 2, (hops - 1) // 2]
    source = [lambda d: (z + hops - d) % hops, lambda d: (z + d) % hops]
    pending = []

    def launch(*args):
        one = copy(*args)
        one.start()
        pending.append(one)

    barrier = pltpu.get_barrier_semaphore()

    def greet(device):
        pl.semaphore_signal(barrier, inc=1, device_id=device, device_id_type=MESH)

    for side in range(2):
        greet(neighbours[side])
    for dy in range(seqs):
        for dt in range(group):
            if dy or dt:
                greet(at(z, (y + dy) % seqs, (tp + dt) % group))

    block = sp
    weights[block, :, 0 * depth : 1 * depth] = wq_ref[...]
    weights[block, :, 1 * depth : 2 * depth] = wk_ref[...]
    weights[block, :, 2 * depth : 3 * depth] = wv_ref[...]
    weights[block, :, 3 * depth : 4 * depth] = wg_ref[...]
    weights[block, :, 4 * depth : 5 * depth] = jnp.broadcast_to(
        wb_ref[...].astype(f32), (wb_ref.shape[0], depth)
    ).astype(bf16)
    small = wo_ref.shape[1]
    unit = jnp.where(iota((small, small), 0) == iota((small, small), 1), 1.0, 0.0)
    weights[block, :, 5 * depth : 6 * depth] = dot(unit, wo_ref[...], NT).astype(bf16)

    pl.semaphore_wait(barrier, 2 + seqs * group - 1)

    for dy in range(1, seqs):
        launch(
            weights.at[block],
            weights.at[block],
            w_send_y.at[dy],
            w_recv.at[0, 0, seqs - dy],
            at(z, (y + dy) % seqs, tp),
        )

    zeros = jnp.zeros((PAD - here_rows, width), f32)
    for seq in range(seqs):
        values = tokens_ref[:, seq, :].astype(f32)
        scaled = values * lax.rsqrt(jnp.mean(values * values, axis=-1, keepdims=True) + epsilon)
        spread[seq] = jnp.concatenate([scaled * in_gain_ref[...], zeros], axis=0).astype(bf16)
    for dy in range(1, seqs):
        to = (y + dy) % seqs
        launch(spread.at[to], strips.at[y], a_send.at[dy], a_recv.at[seqs - dy], at(z, to, tp))
    strips[y] = spread[y]

    def w_copy(side, hop, place, zz, yy):
        one = weights.at[zz * seqs + yy]
        return copy(one, one, w_send_z.at[side, hop, place], w_recv.at[side, hop, place], neighbours[side])

    def w_forward(side, hop, place):
        if hop <= far[side]:
            zz = z if hop == 1 else source[side](hop - 1)
            one = w_copy(side, hop, place, zz, (y + place) % seqs)
            one.start()
            pending.append(one)

    for side in range(2):
        w_forward(side, 1, 0)
    for dy in range(1, seqs):
        yy = (y + dy) % seqs
        slot = weights.at[z * seqs + yy]
        copy(slot, slot, w_send_y.at[dy], w_recv.at[0, 0, dy], me).wait_recv()
        for side in range(2):
            w_forward(side, 1, dy)

    for dy in range(1, seqs):
        slot = strips.at[(y + dy) % seqs]
        copy(slot, slot, a_send.at[dy], a_recv.at[dy], me).wait_recv()
    own_rows = pl.ds(pl.multiple_of(PAD + tp * strip, PAD), strip)
    rows_buf[own_rows, :] = jnp.concatenate(
        [strips[yy].astype(f32)[:here_rows] for yy in range(seqs)], axis=0
    ).astype(bf16)
    for dt in range(1, group):
        launch(
            rows_buf.at[own_rows],
            rows_buf.at[own_rows],
            b_send.at[dt],
            b_recv.at[group - dt],
            at(z, y, (tp + dt) % group),
        )

    def w_hop(hop):
        for place in range(seqs):
            for side in range(2):
                if hop <= far[side]:
                    w_copy(side, hop, place, source[side](hop), (y + place) % seqs).wait_recv()
                    w_forward(side, hop + 1, place)

    middle = max(far) // 2
    for hop in range(1, middle + 1):
        w_hop(hop)
    for dt in range(1, group):
        rows = pl.ds(pl.multiple_of(PAD + (tp + dt) % group * strip, PAD), strip)
        one = rows_buf.at[rows]
        copy(one, one, b_send.at[dt], b_recv.at[dt], me).wait_recv()
    history = copy(
        rows_buf.at[pl.ds(span, PAD)], rows_buf.at[pl.ds(0, PAD)], h_send, h_recv, neighbours[0]
    )
    history.start()
    pending.append(history)
    for hop in range(middle + 1, max(far) + 1):
        w_hop(hop)
    history.wait_recv()

    full = PAD + span
    pre = dot(rows_buf[...], weights[:, :, : 5 * depth].reshape(width, 5 * depth)).astype(bf16)
    row, col = iota((full, full), 0), iota((full, full), 1)
    token, place = row - PAD, col - PAD
    t_of, y_of, i_of = place // strip, place % strip // here_rows, place % here_rows
    match = (token == y_of * (group * here_rows) + t_of * here_rows + i_of) & (place >= 0) & (token >= 0)
    match = match | ((row == col) & (row < PAD) & (z > 0))
    pre = dot(jnp.where(match, 1.0, 0.0), pre)
    conv_buf[...] = pre[:, : 3 * depth]
    gate_pre = pre[PAD:, 3 * depth : 4 * depth]
    shift = math.log(depth / (4.0 * total_tokens))
    beta = jax.nn.sigmoid(pre[PAD:, 4 * depth :] + shift)

    width_taps = taps_ref.shape[0]

    def conv(part, begin):
        columns = slice(part * depth, (part + 1) * depth)
        total = jnp.zeros((size, depth), f32)
        for tap in range(width_taps):
            first = PAD + begin - (width_taps - 1) + tap
            total = total + conv_buf[first : first + size, columns] * taps_ref[tap : tap + 1, columns]
        return total * jax.nn.sigmoid(total)

    rate = rate_ref[0] / total_tokens
    row, col = iota((size, size), 0), iota((size, size), 1)
    decay = jnp.exp(-rate * jnp.maximum(row - col, 0).astype(f32))
    step = iota((size, depth), 0).astype(f32)
    kept = jnp.exp(-rate * (step + 1.0))
    rest = jnp.exp(-rate * (size - 1.0 - step))
    queries, keys, values, betas = [], [], [], []
    for chunk in range(CHUNKS):
        begin = chunk * size
        queries.append(l2_normalize(conv(0, begin)) * depth ** (-0.5))
        keys.append(l2_normalize(conv(1, begin)))
        values.append(conv(2, begin))
        betas.append(beta[begin : begin + size])
    weighted = [k * b for k, b in zip(keys, betas)]
    products = [
        dot(jnp.concatenate([w, q], axis=0), k, NT) for w, q, k in zip(weighted, queries, keys)
    ]
    lowers = [jnp.where(row > col, p[:size] * decay, 0.0) for p in products]
    scores = [jnp.where(row >= col, p[size:] * decay, 0.0) for p in products]
    inverses = unit_inverses(lowers, row, col)
    both = [
        dot(inv, jnp.concatenate([v * b, w * kept], axis=1))
        for inv, v, b, w in zip(inverses, values, betas, weighted)
    ]
    moved = [dot(k * rest, b, TN) for k, b in zip(keys, both)]
    chunk_maps = [(m[:, :depth], m[:, depth:]) for m in moved]
    chunk_kept = jnp.exp(-rate * jnp.full((1, depth), float(size), f32))
    before, before_kept = [], []
    running, running_kept = chunk_maps[0], chunk_kept
    for chunk in range(1, CHUNKS):
        before.append(running)
        before_kept.append(running_kept)
        running = compose(running, running_kept, chunk_maps[chunk], chunk_kept)
        running_kept = running_kept * chunk_kept
    for part in range(2):
        maps[z, part] = running[part].astype(bf16)

    def m_copy(side, hop, part, zz):
        one = maps.at[zz, part]
        return copy(one, one, m_send.at[side, hop, part], m_recv.at[side, hop, part], neighbours[side])

    def m_forward(side, hop, part):
        if hop <= far[side]:
            one = m_copy(side, hop, part, z if hop == 1 else source[side](hop - 1))
            one.start()
            pending.append(one)

    for part in range(2):
        for side in range(2):
            m_forward(side, 1, part)

    reads, locals_ = [], []
    for chunk in range(CHUNKS):
        seen = dot(scores[chunk], both[chunk])
        read = queries[chunk] * kept - seen[:, depth:]
        local = seen[:, :depth]
        if chunk:
            value, erase = before[chunk - 1]
            shifted = dot(read, jnp.concatenate([value, erase], axis=1))
            local = local + shifted[:, :depth]
            read = before_kept[chunk - 1] * read - shifted[:, depth:]
        reads.append(read.astype(bf16))
        locals_.append(local)

    stretch = running_kept
    late, late_kept, early = None, None, jnp.zeros((depth, depth), f32)
    for hop in range(1, max(far) + 1):
        for part in range(2):
            for side in range(2):
                if hop <= far[side]:
                    m_copy(side, hop, part, source[side](hop)).wait_recv()
                    m_forward(side, hop + 1, part)
        zz = source[0](hop)
        value = jnp.where(z >= hop, maps[zz, 0].astype(f32), 0.0)
        erase = maps[zz, 1].astype(f32)
        if late is None:
            late, late_kept = (value, erase), stretch
        else:
            late = compose((value, erase), stretch, late, late_kept)
            late_kept = late_kept * stretch
        if hop <= far[1]:
            zz = source[1](hop)
            new = stretch * early + maps[zz, 0].astype(f32) - dot(maps[zz, 1], early)
            early = jnp.where(z + hop >= hops, new, 0.0)
    state = late[0] + late_kept * early - dot(late[1], early)

    out = jnp.concatenate(locals_, axis=0) + dot(jnp.concatenate(reads, axis=0), state)
    out = out * lax.rsqrt(jnp.mean(out * out, axis=-1, keepdims=True) + out_epsilon)
    gated = (out * out_gain_ref[...] * (gate_pre * jax.nn.sigmoid(gate_pre))).astype(bf16)

    owners = seqs * group
    row, col = iota((owners * PAD, span), 0), iota((owners * PAD, span), 1)
    match = (col == row // PAD * here_rows + row % PAD) & (row % PAD < here_rows)
    gated = dot(jnp.where(match, 1.0, 0.0), gated)
    full_out = weights[:, :, 5 * depth :].reshape(width, depth)
    partial = dot(gated, full_out, NT).astype(bf16)
    parts[...] = partial.reshape(owners, PAD, width)
    mine = y * group + tp
    for dy in range(seqs):
        for dt in range(group):
            if dy or dt:
                yy, tt = (y + dy) % seqs, (tp + dt) % group
                back = (seqs - dy) % seqs * group + (group - dt) % group
                launch(
                    parts.at[yy * group + tt],
                    landed.at[mine],
                    o_send.at[dy * group + dt],
                    o_recv.at[back],
                    at(z, yy, tt),
                )
    landed[mine] = parts[mine]
    for dy in range(seqs):
        for dt in range(group):
            if dy or dt:
                slot = landed.at[(y + dy) % seqs * group + (tp + dt) % group]
                index = dy * group + dt
                copy(slot, slot, o_send.at[index], o_recv.at[index], me).wait_recv()
    for seq in range(seqs):
        total = landed[seq * group].astype(f32)
        for head in range(1, group):
            total = total + landed[seq * group + head].astype(f32)
        out_ref[:, seq, :] = total[:here_rows].astype(bf16)
    for one in pending:
        one.wait_send()


def body(
    tokens,
    in_gain,
    w_query,
    w_key,
    w_value,
    w_gate,
    w_beta,
    conv_query,
    conv_key,
    conv_value,
    decay_rate,
    out_gain,
    w_out,
):
    here_rows, seqs, width = tokens.shape
    depth = w_query.shape[1]
    group, length = lax.axis_size("tp"), lax.axis_size("sp")
    hops = length // seqs
    owners = seqs * group
    span = owners * here_rows
    block = w_query.shape[0]
    taps = jnp.concatenate([conv_query, conv_key, conv_value], axis=1).astype(f32)
    sizes = (depth, seqs, group, hops, here_rows, width)
    vmem = pl.BlockSpec(memory_space=pltpu.VMEM)
    dma = pltpu.SemaphoreType.DMA
    far = hops // 2 + 1
    return pl.pallas_call(
        functools.partial(mixer_kernel, sizes),
        out_shape=jax.ShapeDtypeStruct(tokens.shape, bf16),
        in_specs=[vmem] * 8 + [pl.BlockSpec(memory_space=pltpu.SMEM)] + [vmem] * 2,
        out_specs=vmem,
        scratch_shapes=[
            pltpu.VMEM((length, block, 6 * depth), bf16),
            pltpu.VMEM((seqs, PAD, width), bf16),
            pltpu.VMEM((seqs, PAD, width), bf16),
            pltpu.VMEM((PAD + span, width), bf16),
            pltpu.VMEM((PAD + span, 3 * depth), f32),
            pltpu.VMEM((hops, 2, depth, depth), bf16),
            pltpu.VMEM((owners, PAD, width), bf16),
            pltpu.VMEM((owners, PAD, width), bf16),
            dma((seqs,)),
            dma((2, far, seqs)),
            dma((2, far, seqs)),
            dma((seqs,)),
            dma((seqs,)),
            dma((group,)),
            dma((group,)),
            dma,
            dma,
            dma((2, far, 2)),
            dma((2, far, 2)),
            dma((owners,)),
            dma((owners,)),
        ],
        compiler_params=pltpu.CompilerParams(
            collective_id=0, has_side_effects=True, vmem_limit_bytes=48 * 1024 * 1024
        ),
    )(
        tokens,
        in_gain[None],
        w_query,
        w_key,
        w_value,
        w_gate,
        w_beta,
        taps,
        decay_rate,
        out_gain[None],
        w_out,
    )


def solution(mesh):
    placed = (
        P(("sp", "tp"), None, None),
        P(),
        P("sp", "tp"),
        P("sp", "tp"),
        P("sp", "tp"),
        P("sp", "tp"),
        P("sp", "tp"),
        P(None, "tp"),
        P(None, "tp"),
        P(None, "tp"),
        P("tp"),
        P(),
        P("tp", "sp"),
    )
    return jax.shard_map(
        body, mesh=mesh, in_specs=placed, out_specs=P(("sp", "tp"), None, None), check_vma=False
    )
```

time: 527 us -> 95.9 us (0.18)
  waiting for transfers between devices: 303 us -> 0 us
  blocking collectives: 96.4 us -> 0 us
  Pallas kernels: 13.5 us -> 90.4 us
  local copies, waits for them, and re-layouts: 72.4 us -> 4.3 us
  matrix products: 15.5 us -> 0 us
  between operations: 14.6 us -> 0.7 us
    all_gather x2 -> x0, waiting for transfers between devices: 232 us -> none  [the longest x1 123 us: incoming_states(): everything = lax.all_gather(maps, 'sp')]
    all_gather x2 -> x0, blocking collectives: 96.4 us -> none  [the longest x1 76.3 us: body(): full_out = lax.all_gather(w_out.T, 'sp', axis=0, tiled=True)]
    pallas_call x2 -> x1, Pallas kernels: 13.5 us -> 90.4 us  [body(): pl.pallas_call(functools.partial(mixer_kernel, sizes), out_shape=jax.Shap...]
    unnamed x4 -> x0, waiting for transfers between devices: 71.3 us -> none
    convert_element_type x65 -> x0, local copies, waits for them, and re-layouts: 63.9 us -> none  [the longest x64 62.3 us: hop(): moved = everything[index].astype(f32)]
    dot_general x66 -> x0, matrix products: 15.5 us -> none  [the longest x64 11.3 us: hop(): jnp.einsum('pde,pev->pdv', moved[:, :, depth:].astype(bf16), state.astype...]
  transfers between devices with their start and end apart: 4 -> 0, of which waited for: 3 -> 0; matrix products, arithmetic and copies ran while one was open for 1% -> 0% of each run, Pallas kernels for 0% -> 0%
where the time goes in v1:
time: 95.9 us; the launch traced here: 95.4 us
  Pallas kernels  90.4 us (94%)
  local copies, waits for them, and re-layouts  4.3 us (4%)
    pallas_call x1, Pallas kernels, body(): pl.pallas_call(functools.partial(mixer_kernel, sizes), out_shape=jax.Shap...  90.4 us
    unnamed x27, local copies, waits for them, and re-layouts  4.3 us

profile of v1, /device:TPU:1, one launch (start us, length us, event | category | flops | bytes accessed | tf_op | source)
XLA Modules:
  0.0 95.4 jit_solution(18159633828625839787)
XLA Ops:
  0.7 0.0 copy-start.11
  0.7 0.6 copy-done.11
  1.3 0.0 copy-start.8
  1.3 0.0 copy-start.9
  1.3 0.0 copy-start.10
  1.3 0.1 copy.14.wb_ref
  1.4 0.6 copy-done.8
  2.0 0.0 copy-done.9
  2.0 0.0 copy-done.10
  2.0 0.0 copy-start.7
  2.0 0.7 copy-done.7
  2.7 0.0 copy-start.1
  2.7 0.0 copy-start.2
  2.7 0.0 copy-start.3
  2.7 0.0 copy-start.4
  2.7 0.0 copy-start.5
  2.7 0.0 copy-start.6
  2.7 0.1 copy.15.wo_ref
  2.9 0.5 copy-done.1
  3.4 0.0 copy-done.2
  3.4 0.0 copy-done.3
  3.4 0.0 copy-done.4
  3.4 0.0 copy-done.5
  3.5 0.0 copy-done.6
  3.5 0.0 copy-start
  3.5 0.9 copy-done
  4.4 90.4 %shard_map.127 = bf16[12,4,1024]{2,1,0:T(4,128)(2,1)S(1)} custom-call(bf16[12,4,1024]{2,1,0:T(4,128)(2,1)S(1)} %copy-done, f32[1,1024]{1,0:T(1,128)S(1)} %bitcast.2, bf16[16,128]{1,0:T(8,128)(2,1)S(1)} %copy-done.2, bf16[16,128]{1,0:T(8,128)(2,1)S(1)} %copy-done.3, bf16[16,128]{1,0:T(8,128)(2,1)S(1)} %copy-done.4, bf16[16,128]{1,0:T(8,128)(2,1)S(1)} %copy-done.5, ...), custom_call_target="tpu_custom_call" | custom-call | tf_op jit(solution)/shard_map/pallas_call | solution.py:406
  94.7 0.6 copy.18
  (1 shorter events, 0.0 us)
Async XLA Ops:
  0.7 0.7 copy-start.11
  1.3 0.7 copy-start.8
  1.3 0.7 copy-start.9
  1.3 0.7 copy-start.10
  2.0 0.7 copy-start.7
  2.7 0.7 copy-start.1
  2.7 0.7 copy-start.2
  2.7 0.7 copy-start.3
  2.7 0.7 copy-start.4
  2.7 0.7 copy-start.5
  2.7 0.7 copy-start.6
  3.5 0.9 copy-start

commit v2 on v1

v2 whole, which is shorter than its diff:
```python
import functools
import math

import jax
import jax.numpy as jnp
from jax import lax
from jax.experimental import pallas as pl
from jax.experimental.pallas import tpu as pltpu
from jax.sharding import PartitionSpec as P

MESH = pl.DeviceIdType.MESH
PAD = 16
CHUNKS = 3
CORES = 2
REACH = 4
epsilon = 1e-06
out_epsilon = 1e-10
f32 = jnp.float32
bf16 = jnp.bfloat16
NN, NT, TN = ((1,), (0,)), ((1,), (1,)), ((0,), (0,))


def dot(a, b, dims=NN):
    return lax.dot_general(
        a.astype(bf16), b.astype(bf16), (dims, ((), ())), preferred_element_type=f32
    )


def iota(shape, axis):
    return lax.broadcasted_iota(jnp.int32, shape, axis)


def l2_normalize(array):
    return array * lax.rsqrt(jnp.sum(array * array, axis=-1, keepdims=True) + epsilon)


def unit_inverses(lowers, row, col):
    size = row.shape[0]
    near = ((row >> 1) == (col >> 1)) & (row != col)
    eye = jnp.where(row == col, 1.0, 0.0)
    inverses = [eye - jnp.where(near, lower, 0.0) for lower in lowers]
    level = 1
    while (1 << level) < size:
        mask = ((row >> (level + 1)) == (col >> (level + 1))) & ((row >> level) != (col >> level))
        inner = [dot(jnp.where(mask, l, 0.0), v) for l, v in zip(lowers, inverses)]
        inverses = [v - dot(v, w) for v, w in zip(inverses, inner)]
        level += 1
    return inverses


def compose(first, kept_first, second, kept_second):
    depth = first[0].shape[0]
    cross = dot(second[1], jnp.concatenate(first, axis=1))
    value = kept_second * first[0] + second[0] - cross[:, :depth]
    erase = kept_second * first[1] + kept_first * second[1] - cross[:, depth:]
    return value, erase


def mixer_kernel(
    sizes,
    tokens_hbm,
    in_gain_hbm,
    wq_hbm,
    wk_hbm,
    wv_hbm,
    wg_hbm,
    wb_hbm,
    cq_hbm,
    ck_hbm,
    cv_hbm,
    rate_ref,
    out_gain_hbm,
    wo_hbm,
    out_ref,
    tokens_ref,
    in_gain_ref,
    beta_ref,
    cq_ref,
    ck_ref,
    cv_ref,
    out_gain_ref,
    first_half,
    second_half,
    spread,
    rows_buf,
    conv_buf,
    maps,
    swap_out,
    swap_in,
    parts,
    landed,
    load,
    z_send,
    z_recv,
    y_send,
    y_recv,
    q_send,
    q_recv,
    t_send,
    t_recv,
    c_send,
    c_recv,
    h_send,
    h_recv,
    m_send,
    m_recv,
    s_send,
    s_recv,
    o_send,
    o_recv,
):
    depth, seqs, group, hops, here_rows, width = sizes
    chips = group // CORES
    total_tokens = hops * seqs * group * here_rows
    span = seqs * group * here_rows
    size = span // CHUNKS
    sp, tp = lax.axis_index("sp"), lax.axis_index("tp")
    z, y = sp // seqs, sp % seqs
    x, core = tp // CORES, tp % CORES
    far = [hops // 2, (hops - 1) // 2]
    halves = [first_half, second_half]
    pending = []

    def at(dz, dy, dx, dc=0):
        return {
            "sp": (z + dz) % hops * seqs + (y + dy) % seqs,
            "tp": (x + dx) % chips * CORES + (core + dc) % CORES,
        }

    def copy(src, dst, send, recv, device):
        return pltpu.make_async_remote_copy(
            src_ref=src,
            dst_ref=dst,
            send_sem=send,
            recv_sem=recv,
            device_id=device,
            device_id_type=MESH,
        )

    me = {"sp": sp, "tp": tp}
    partner = at(0, 0, 0, 1)

    def launch(*args):
        one = copy(*args)
        one.start()
        pending.append(one)

    barrier = pltpu.get_barrier_semaphore()
    plane = [(dy, dx) for dy in range(seqs) for dx in range(chips) if dy or dx]
    reach = [d for d in range(1, REACH + 1) if d <= far[0]]
    reach_back = [d for d in range(1, REACH + 1) if d <= far[1]]
    friends = [partner] + [at(0, dy, dx) for dy, dx in plane]
    friends += [at(d, 0, 0) for d in reach] + [at(hops - d, 0, 0) for d in reach]
    for device in friends:
        pl.semaphore_signal(barrier, inc=1, device_id=device, device_id_type=MESH)

    def own(half, part):
        return halves[half].at[z, y, :, pl.ds(part * depth, depth)]

    loads = [
        (tokens_hbm, tokens_ref),
        (in_gain_hbm, in_gain_ref),
        (wk_hbm, own(0, 0)),
        (wv_hbm, own(0, 1)),
        (wb_hbm, beta_ref),
        (wq_hbm, own(1, 0)),
        (wg_hbm, own(1, 1)),
        (wo_hbm, own(1, 2)),
        (cq_hbm, cq_ref),
        (ck_hbm, ck_ref),
        (cv_hbm, cv_ref),
        (out_gain_hbm, out_gain_ref),
    ]
    loads = [pltpu.make_async_copy(a, b, load.at[i]) for i, (a, b) in enumerate(loads)]
    for one in loads:
        one.start()
    for one in loads:
        one.wait()

    block = wk_hbm.shape[0]
    unit = jnp.where(iota((block, block), 0) == iota((block, block), 1), 1.0, 0.0)
    column = jnp.broadcast_to(beta_ref[...].astype(f32), (depth, block))
    first_half[z, y, :, 2 * depth :] = dot(unit, column, NT).astype(bf16)

    pad_rows = jnp.zeros((PAD - here_rows, width), f32)
    for seq in range(seqs):
        values = tokens_ref[:, seq, :].astype(f32)
        scaled = values * lax.rsqrt(jnp.mean(values * values, axis=-1, keepdims=True) + epsilon)
        spread[seq] = jnp.concatenate([scaled * in_gain_ref[...], pad_rows], axis=0).astype(bf16)

    pl.semaphore_wait(barrier, len(friends))

    def z_copy(half, index, offset, device):
        one = halves[half].at[(z + offset) % hops, y]
        return copy(one, one, z_send.at[half, index], z_recv.at[half, index], device)

    def z_launch(half, index, offset, device):
        one = z_copy(half, index, offset, device)
        one.start()
        pending.append(one)

    def offset_of(index):
        return hops - index if index <= far[0] else index - far[0]

    def z_first(half):
        for d in reversed(reach):
            z_launch(half, d, 0, at(d, 0, 0))
            if d in reach_back:
                z_launch(half, far[0] + d, 0, at(hops - d, 0, 0))

    def z_arrived(half, index):
        z_copy(half, index, offset_of(index), me).wait_recv()

    def z_relay(half):
        for further in range(far[0] - REACH):
            if further == 0:
                z_arrived(half, REACH)
            index = far[0] - further
            z_launch(half, index, hops - REACH, at(index - REACH, 0, 0))
        for further in range(far[1] - REACH):
            if further == 0:
                z_arrived(half, far[0] + REACH)
            d = far[1] - further
            z_launch(half, far[0] + d, REACH, at(hops - (d - REACH), 0, 0))

    def y_copy(index, dy, offset, yy, device, back=None):
        one = first_half.at[(z + offset) % hops, yy]
        back = dy if back is None else back
        return copy(one, one, y_send.at[index, dy], y_recv.at[index, back], device)

    def y_fan(index):
        offset = offset_of(index) if index else 0
        for dy in (2, 1, 3):
            one = y_copy(index, dy, offset, y, at(0, dy, 0), seqs - dy)
            one.start()
            pending.append(one)

    def t_slot(yy, xx, cc):
        return rows_buf.at[1 + (yy * chips + xx) * CORES + cc]

    relayed = far[0] > REACH
    z_first(0)
    for index, (dy, dx) in enumerate(plane):
        launch(
            spread.at[(y + dy) % seqs],
            t_slot(y, x, core),
            t_send.at[index],
            t_recv.at[(seqs - dy) % seqs * chips + (chips - dx) % chips],
            at(0, dy, dx),
        )
    y_fan(0)
    launch(spread.at[y], t_slot(y, x, core), c_send.at[0], c_recv.at[0], partner)
    rows_buf[1 + (y * chips + x) * CORES + core] = spread[y]
    z_first(1)

    if relayed:
        z_relay(0)
        y_fan(REACH)
        y_fan(far[0] + REACH)
    for d in range(1, REACH if relayed else REACH + 1):
        for index in [d, far[0] + d]:
            if d <= far[index > far[0]]:
                z_arrived(0, index)
                y_fan(index)
    for dy, dx in plane:
        index = dy * chips + dx
        slot = t_slot((y + dy) % seqs, (x + dx) % chips, core)
        copy(slot, slot, t_send.at[0], t_recv.at[index], me).wait_recv()
        launch(slot, slot, c_send.at[index], c_recv.at[index], partner)
    if relayed:
        for d in range(REACH + 1, far[0] + 1):
            for index in [d, far[0] + d]:
                if d <= far[index > far[0]]:
                    z_arrived(0, index)
                    y_fan(index)
        z_relay(1)
    for dy, dx in [(0, 0)] + plane:
        index = dy * chips + dx
        slot = t_slot((y + dy) % seqs, (x + dx) % chips, (core + 1) % CORES)
        copy(slot, slot, c_send.at[0], c_recv.at[index], me).wait_recv()
    history = copy(rows_buf.at[seqs * group], rows_buf.at[0], h_send, h_recv, at(1, 0, 0))
    history.start()
    pending.append(history)
    for d in range(1, far[0] + 1):
        for index in [d, far[0] + d]:
            if d <= far[index > far[0]] and not (relayed and d == REACH):
                z_arrived(1, index)
    for dy in (2, 1, 3):
        one = second_half.at[:, y]
        launch(one, one, q_send.at[dy], q_recv.at[seqs - dy], at(0, dy, 0))
    for index in range(far[0] + far[1] + 1):
        offset = offset_of(index) if index else 0
        for dy in (1, 3, 2):
            y_copy(index, dy, offset, (y + dy) % seqs, me).wait_recv()
    history.wait_recv()

    full = PAD + span
    padded = (1 + seqs * group) * PAD
    row, col = iota((full, padded), 0), iota((full, padded), 1)
    place, inside = col // PAD, col % PAD
    select = (row == PAD + (place - 1) * here_rows + inside) & (inside < here_rows)
    select = jnp.where(select & ((place > 0) | (z > 0)), 1.0, 0.0).astype(bf16)

    def project(half, columns):
        weights = half[:, :, :, :columns].reshape(width, columns)
        pre = dot(rows_buf[...].reshape(padded, width), weights).astype(bf16)
        return dot(select, pre)

    pre = project(first_half, 3 * depth)
    conv_buf[:, : 2 * depth] = pre[:, : 2 * depth]
    shift = math.log(depth / (4.0 * total_tokens))
    beta = jax.nn.sigmoid(pre[PAD:, 2 * depth :] + shift)
    width_taps = cq_ref.shape[0]

    def conv(part, taps_ref, begin):
        columns = slice(part * depth, (part + 1) * depth)
        total = jnp.zeros((size, depth), f32)
        for tap in range(width_taps):
            first = PAD + begin - (width_taps - 1) + tap
            taps = taps_ref[tap : tap + 1, :].astype(f32)
            total = total + conv_buf[first : first + size, columns] * taps
        return total * jax.nn.sigmoid(total)

    rate = rate_ref[0] / total_tokens
    row, col = iota((size, size), 0), iota((size, size), 1)
    decay = jnp.exp(-rate * jnp.maximum(row - col, 0).astype(f32))
    step = iota((size, depth), 0).astype(f32)
    kept = jnp.exp(-rate * (step + 1.0))
    rest = jnp.exp(-rate * (size - 1.0 - step))
    keys, values, betas = [], [], []
    for chunk in range(CHUNKS):
        begin = chunk * size
        keys.append(l2_normalize(conv(0, ck_ref, begin)))
        values.append(conv(1, cv_ref, begin))
        betas.append(beta[begin : begin + size])
    weighted = [k * b for k, b in zip(keys, betas)]
    lowers = [
        jnp.where(row > col, dot(w, k, NT) * decay, 0.0) for w, k in zip(weighted, keys)
    ]
    inverses = unit_inverses(lowers, row, col)
    both = [
        dot(inv, jnp.concatenate([v * b, w * kept], axis=1))
        for inv, v, b, w in zip(inverses, values, betas, weighted)
    ]
    moved = [dot(k * rest, b, TN) for k, b in zip(keys, both)]
    chunk_maps = [(m[:, :depth], m[:, depth:]) for m in moved]
    chunk_kept = jnp.exp(-rate * jnp.full((1, depth), float(size), f32))
    before, before_kept = [], []
    running, running_kept = chunk_maps[0], chunk_kept
    for chunk in range(1, CHUNKS):
        before.append(running)
        before_kept.append(running_kept)
        running = compose(running, running_kept, chunk_maps[chunk], chunk_kept)
        running_kept = running_kept * chunk_kept
    for part in range(2):
        maps[z, part] = running[part].astype(bf16)

    source = [lambda d: (z + hops - d) % hops, lambda d: (z + d) % hops]
    neighbours = [at(1, 0, 0), at(hops - 1, 0, 0)]

    def m_copy(side, hop, part, zz):
        one = maps.at[zz, part]
        return copy(one, one, m_send.at[side, hop, part], m_recv.at[side, hop, part], neighbours[side])

    def m_forward(side, hop, part):
        if hop <= far[side]:
            one = m_copy(side, hop, part, z if hop == 1 else source[side](hop - 1))
            one.start()
            pending.append(one)

    for part in range(2):
        for side in range(2):
            m_forward(side, 1, part)

    late_work = {}

    def project_second():
        for dy in (1, 3, 2):
            one = second_half.at[:, (y + dy) % seqs]
            copy(one, one, q_send.at[dy], q_recv.at[dy], me).wait_recv()
        pre = project(second_half, 2 * depth)
        conv_buf[:, : depth] = pre[:, :depth]
        gate_pre = pre[PAD:, depth:]
        late_work["gate"] = gate_pre * jax.nn.sigmoid(gate_pre)

    def queries_and_scores():
        queries = [
            l2_normalize(conv(0, cq_ref, chunk * size)) * depth ** (-0.5) for chunk in range(CHUNKS)
        ]
        late_work["queries"] = queries
        late_work["scores"] = [
            jnp.where(row >= col, dot(q, k, NT) * decay, 0.0) for q, k in zip(queries, keys)
        ]

    def reads_and_locals():
        reads, locals_ = [], []
        for chunk in range(CHUNKS):
            seen = dot(late_work["scores"][chunk], both[chunk])
            read = late_work["queries"][chunk] * kept - seen[:, depth:]
            local = seen[:, :depth]
            if chunk:
                value, erase = before[chunk - 1]
                shifted = dot(read, jnp.concatenate([value, erase], axis=1))
                local = local + shifted[:, :depth]
                read = before_kept[chunk - 1] * read - shifted[:, depth:]
            reads.append(read.astype(bf16))
            locals_.append(local)
        late_work["reads"], late_work["locals"] = reads, locals_

    beside = [project_second, queries_and_scores, reads_and_locals]
    first_beside = max(1, far[0] - 3)

    stretch = running_kept
    late, late_kept, early = None, None, jnp.zeros((depth, depth), f32)
    for hop in range(1, far[0] + 1):
        for part in range(2):
            for side in range(2):
                if hop <= far[side]:
                    m_copy(side, hop, part, source[side](hop)).wait_recv()
                    m_forward(side, hop + 1, part)
        zz = source[0](hop)
        value = jnp.where(z >= hop, maps[zz, 0].astype(f32), 0.0)
        erase = maps[zz, 1].astype(f32)
        if late is None:
            late, late_kept = (value, erase), stretch
        else:
            late = compose((value, erase), stretch, late, late_kept)
            late_kept = late_kept * stretch
        if hop <= far[1]:
            zz = source[1](hop)
            new = stretch * early + maps[zz, 0].astype(f32) - dot(maps[zz, 1], early)
            early = jnp.where(z + hop >= hops, new, 0.0)
        if hop >= first_beside and beside:
            beside.pop(0)()
    for one in beside:
        one()
    state = late[0] + late_kept * early - dot(late[1], early)

    out = jnp.concatenate(late_work["locals"], axis=0)
    out = out + dot(jnp.concatenate(late_work["reads"], axis=0), state)
    out = out * lax.rsqrt(jnp.mean(out * out, axis=-1, keepdims=True) + out_epsilon)
    gated = (out * out_gain_ref[...] * late_work["gate"]).astype(bf16)

    full_out = second_half[:, :, :, 2 * depth :].reshape(width, depth)
    order = [2, 1, 3, 0]
    batch = chips * PAD
    row, col = iota((batch, span), 0), iota((batch, span), 1)

    def owned_by(dy, cc):
        owner = ((y + dy) % seqs * chips + row // PAD) * CORES + cc
        match = (col == owner * here_rows + row % PAD) & (row % PAD < here_rows)
        return jnp.where(match, 1.0, 0.0)

    def products(cc):
        rows = dot(jnp.concatenate([owned_by(dy, cc) for dy in order], axis=0), gated)
        return dot(rows, full_out, NT)

    theirs = products(1 - core).astype(bf16)
    for i in range(seqs):
        swap_out[i] = theirs[i * batch : (i + 1) * batch].reshape(chips, PAD, width)
        launch(swap_out.at[i], swap_in.at[i], s_send.at[i], s_recv.at[i], partner)
    mine = products(core)
    for i, dy in enumerate(order):
        copy(swap_in.at[i], swap_in.at[i], s_send.at[i], s_recv.at[i], me).wait_recv()
        total = mine[i * batch : (i + 1) * batch].reshape(chips, PAD, width) + swap_in[i].astype(f32)
        parts[i] = total.astype(bf16)
        for dx in range(chips):
            if dy or dx:
                launch(
                    parts.at[i, (x + dx) % chips],
                    landed.at[y * chips + x],
                    o_send.at[dy * chips + dx],
                    o_recv.at[(seqs - dy) % seqs * chips + (chips - dx) % chips],
                    at(0, dy, dx),
                )
    landed[y * chips + x] = parts[seqs - 1, x]
    for dy, dx in plane:
        slot = landed.at[(y + dy) % seqs * chips + (x + dx) % chips]
        index = dy * chips + dx
        copy(slot, slot, o_send.at[index], o_recv.at[index], me).wait_recv()
    for seq in range(seqs):
        total = landed[seq * chips].astype(f32)
        for chip in range(1, chips):
            total = total + landed[seq * chips + chip].astype(f32)
        out_ref[:, seq, :] = total[:here_rows].astype(bf16)
    for one in pending:
        one.wait_send()


def body(
    tokens,
    in_gain,
    w_query,
    w_key,
    w_value,
    w_gate,
    w_beta,
    conv_query,
    conv_key,
    conv_value,
    decay_rate,
    out_gain,
    w_out,
):
    here_rows, seqs, width = tokens.shape
    depth = w_query.shape[1]
    group, length = lax.axis_size("tp"), lax.axis_size("sp")
    hops = length // seqs
    chips = group // CORES
    owners = seqs * group
    span = owners * here_rows
    block = w_query.shape[0]
    sizes = (depth, seqs, group, hops, here_rows, width)
    anywhere = pl.BlockSpec(memory_space=pl.ANY)
    dma = pltpu.SemaphoreType.DMA
    vmem = pltpu.VMEM
    far = hops // 2 + 1
    return pl.pallas_call(
        functools.partial(mixer_kernel, sizes),
        out_shape=jax.ShapeDtypeStruct(tokens.shape, bf16),
        in_specs=[anywhere] * 10 + [pl.BlockSpec(memory_space=pltpu.SMEM)] + [anywhere] * 2,
        out_specs=pl.BlockSpec(memory_space=vmem),
        scratch_shapes=[
            vmem(tokens.shape, bf16),
            vmem((1, width), f32),
            vmem((1, block), bf16),
            vmem(conv_query.shape, bf16),
            vmem(conv_query.shape, bf16),
            vmem(conv_query.shape, bf16),
            vmem((1, depth), f32),
            vmem((hops, seqs, block, 3 * depth), bf16),
            vmem((hops, seqs, block, 3 * depth), bf16),
            vmem((seqs, PAD, width), bf16),
            vmem((1 + owners, PAD, width), bf16),
            vmem((PAD + span, 2 * depth), f32),
            vmem((hops, 2, depth, depth), bf16),
            vmem((seqs, chips, PAD, width), bf16),
            vmem((seqs, chips, PAD, width), bf16),
            vmem((seqs, chips, PAD, width), bf16),
            vmem((seqs * chips, PAD, width), bf16),
            dma((12,)),
            dma((2, hops)),
            dma((2, hops)),
            dma((hops, seqs)),
            dma((hops, seqs)),
            dma((seqs,)),
            dma((seqs,)),
            dma((seqs * chips,)),
            dma((seqs * chips,)),
            dma((seqs * chips,)),
            dma((seqs * chips,)),
            dma,
            dma,
            dma((2, far, 2)),
            dma((2, far, 2)),
            dma((seqs,)),
            dma((seqs,)),
            dma((seqs * chips,)),
            dma((seqs * chips,)),
        ],
        compiler_params=pltpu.CompilerParams(
            collective_id=0, has_side_effects=True, vmem_limit_bytes=56 * 1024 * 1024
        ),
    )(
        tokens,
        in_gain[None],
        w_query,
        w_key,
        w_value,
        w_gate,
        w_beta.T,
        conv_query,
        conv_key,
        conv_value,
        decay_rate,
        out_gain[None],
        w_out.T,
    )


def solution(mesh):
    placed = (
        P(("sp", "tp"), None, None),
        P(),
        P("sp", "tp"),
        P("sp", "tp"),
        P("sp", "tp"),
        P("sp", "tp"),
        P("sp", "tp"),
        P(None, "tp"),
        P(None, "tp"),
        P(None, "tp"),
        P("tp"),
        P(),
        P("tp", "sp"),
    )
    return jax.shard_map(
        body, mesh=mesh, in_specs=placed, out_specs=P(("sp", "tp"), None, None), check_vma=False
    )
```

time: 95.9 us -> 80.4 us (0.84)
  Pallas kernels: 90.4 us -> 78 us
  local copies, waits for them, and re-layouts: 4.3 us -> 1.57 us
    pallas_call x1, Pallas kernels: 90.4 us -> 78 us  [body(): pl.pallas_call(functools.partial(mixer_kernel, sizes), out_shape=jax.Shap...]
    unnamed x27 -> x1, local copies, waits for them, and re-layouts: 4.3 us -> 1.57 us
where the time goes in v2:
time: 80.4 us; the launch traced here: 80.2 us
  Pallas kernels  78 us (97%)
  local copies, waits for them, and re-layouts  1.57 us (2%)
    pallas_call x1, Pallas kernels, body(): pl.pallas_call(functools.partial(mixer_kernel, sizes), out_shape=jax.Shap...  78 us

profile of v2, /device:TPU:1, one launch (start us, length us, event | category | flops | bytes accessed | tf_op | source)
XLA Modules:
  0.0 80.2 jit_solution(3499047596412025328)
XLA Ops:
  0.7 78.0 %shard_map.127 = bf16[12,4,1024]{2,1,0:T(4,128)(2,1)} custom-call(bf16[12,4,1024]{2,1,0:T(4,128)(2,1)} %tokens_hbm.1, f32[1,1024]{1,0:T(1,128)} %bitcast.4, bf16[16,128]{1,0:T(8,128)(2,1)} %wq_hbm.1, bf16[16,128]{1,0:T(8,128)(2,1)} %wk_hbm.1, bf16[16,128]{1,0:T(8,128)(2,1)} %wv_hbm.1, bf16[16,128]{1,0:T(8,128)(2,1)} %wg_hbm.1, bf16[1,16]{1,0:T(2,128)(2,1)} %bitcast.6, ...), custom_call_target="tpu_custom_call" | custom-call | tf_op jit(solution)/shard_map/pallas_call | solution.py:518
  78.6 1.6 %copy.16 = bf16[12,4,1024]{2,1,0:T(4,128)(2,1)} copy(bf16[12,4,1024]{2,1,0:T(4,128)(2,1)} %shard_map.127) | data formatting | bytes 196608

commit v3 on v2

--- a/solution.py
+++ b/solution.py
@@ -13,6 +13,7 @@
 CHUNKS = 3
 CORES = 2
 REACH = 4
+FIRST_BESIDE = 4
 epsilon = 1e-06
 out_epsilon = 1e-10
 f32 = jnp.float32
@@ -281,13 +282,6 @@
     history = copy(rows_buf.at[seqs * group], rows_buf.at[0], h_send, h_recv, at(1, 0, 0))
     history.start()
     pending.append(history)
-    for d in range(1, far[0] + 1):
-        for index in [d, far[0] + d]:
-            if d <= far[index > far[0]] and not (relayed and d == REACH):
-                z_arrived(1, index)
-    for dy in (2, 1, 3):
-        one = second_half.at[:, y]
-        launch(one, one, q_send.at[dy], q_recv.at[seqs - dy], at(0, dy, 0))
     for index in range(far[0] + far[1] + 1):
         offset = offset_of(index) if index else 0
         for dy in (1, 3, 2):
@@ -356,21 +350,36 @@
         maps[z, part] = running[part].astype(bf16)
 
     source = [lambda d: (z + hops - d) % hops, lambda d: (z + d) % hops]
-    neighbours = [at(1, 0, 0), at(hops - 1, 0, 0)]
-
-    def m_copy(side, hop, part, zz):
-        one = maps.at[zz, part]
-        return copy(one, one, m_send.at[side, hop, part], m_recv.at[side, hop, part], neighbours[side])
-
-    def m_forward(side, hop, part):
-        if hop <= far[side]:
-            one = m_copy(side, hop, part, z if hop == 1 else source[side](hop - 1))
-            one.start()
-            pending.append(one)
-
-    for part in range(2):
-        for side in range(2):
-            m_forward(side, 1, part)
+
+    def m_copy(side, hop, part, offset, device):
+        one = maps.at[source[side](offset), part]
+        return copy(one, one, m_send.at[side, hop, part], m_recv.at[side, hop, part], device)
+
+    def m_forward(behind):
+        for step in (2, 1):
+            for part in range(2):
+                for side in range(2):
+                    if behind + step <= far[side]:
+                        device = at(step if side == 0 else hops - step, 0, 0)
+                        one = m_copy(side, behind + step, part, behind, device)
+                        one.start()
+                        pending.append(one)
+
+    def m_arrived(hop):
+        for part in range(2):
+            for side in range(2):
+                if hop <= far[side]:
+                    m_copy(side, hop, part, hop, me).wait_recv()
+
+    m_forward(0)
+
+    for d in range(1, far[0] + 1):
+        for index in [d, far[0] + d]:
+            if d <= far[index > far[0]] and not (relayed and d == REACH):
+                z_arrived(1, index)
+    for dy in (2, 1, 3):
+        one = second_half.at[:, y]
+        launch(one, one, q_send.at[dy], q_recv.at[seqs - dy], at(0, dy, 0))
 
     late_work = {}
 
@@ -408,29 +417,30 @@
         late_work["reads"], late_work["locals"] = reads, locals_
 
     beside = [project_second, queries_and_scores, reads_and_locals]
-    first_beside = max(1, far[0] - 3)
-
     stretch = running_kept
     late, late_kept, early = None, None, jnp.zeros((depth, depth), f32)
-    for hop in range(1, far[0] + 1):
-        for part in range(2):
-            for side in range(2):
-                if hop <= far[side]:
-                    m_copy(side, hop, part, source[side](hop)).wait_recv()
-                    m_forward(side, hop + 1, part)
-        zz = source[0](hop)
-        value = jnp.where(z >= hop, maps[zz, 0].astype(f32), 0.0)
-        erase = maps[zz, 1].astype(f32)
-        if late is None:
-            late, late_kept = (value, erase), stretch
-        else:
-            late = compose((value, erase), stretch, late, late_kept)
-            late_kept = late_kept * stretch
-        if hop <= far[1]:
-            zz = source[1](hop)
-            new = stretch * early + maps[zz, 0].astype(f32) - dot(maps[zz, 1], early)
-            early = jnp.where(z + hop >= hops, new, 0.0)
-        if hop >= first_beside and beside:
+    for stage in range(2, far[0] + 2, 2):
+        if stage <= far[0]:
+            m_arrived(stage)
+            m_forward(stage)
+        for hop in (stage - 1, stage):
+            if hop > far[0]:
+                continue
+            if hop < stage:
+                m_arrived(hop)
+            zz = source[0](hop)
+            value = jnp.where(z >= hop, maps[zz, 0].astype(f32), 0.0)
+            erase = maps[zz, 1].astype(f32)
+            if late is None:
+                late, late_kept = (value, erase), stretch
+            else:
+                late = compose((value, erase), stretch, late, late_kept)
+                late_kept = late_kept * stretch
+            if hop <= far[1]:
+                zz = source[1](hop)
+                new = stretch * early + maps[zz, 0].astype(f32) - dot(maps[zz, 1], early)
+                early = jnp.where(z + hop >= hops, new, 0.0)
+        if stage >= FIRST_BESIDE and beside:
             beside.pop(0)()
     for one in beside:
         one()

time: 80.4 us -> 75 us (0.933)
  Pallas kernels: 78 us -> 72.6 us
    pallas_call x1, Pallas kernels: 78 us -> 72.6 us  [body(): pl.pallas_call(functools.partial(mixer_kernel, sizes), out_shape=jax.Shap...]
where the time goes in v3:
time: 75 us; the launch traced here: 74.8 us
  Pallas kernels  72.6 us (97%)
  local copies, waits for them, and re-layouts  1.57 us (2%)
    pallas_call x1, Pallas kernels, body(): pl.pallas_call(functools.partial(mixer_kernel, sizes), out_shape=jax.Shap...  72.6 us
    unnamed x1, local copies, waits for them, and re-layouts  1.57 us

profile of v3, /device:TPU:1, one launch (start us, length us, event | category | flops | bytes accessed | tf_op | source)
XLA Modules:
  0.0 74.8 jit_solution(9407845495024110899)
XLA Ops:
  0.7 72.6 %shard_map.127 = bf16[12,4,1024]{2,1,0:T(4,128)(2,1)} custom-call(bf16[12,4,1024]{2,1,0:T(4,128)(2,1)} %tokens_hbm.1, f32[1,1024]{1,0:T(1,128)} %bitcast.4, bf16[16,128]{1,0:T(8,128)(2,1)} %wq_hbm.1, bf16[16,128]{1,0:T(8,128)(2,1)} %wk_hbm.1, bf16[16,128]{1,0:T(8,128)(2,1)} %wv_hbm.1, bf16[16,128]{1,0:T(8,128)(2,1)} %wg_hbm.1, bf16[1,16]{1,0:T(2,128)(2,1)} %bitcast.6, ...), custom_call_target="tpu_custom_call" | custom-call | tf_op jit(solution)/shard_map/pallas_call | solution.py:528
  73.2 1.6 %copy.16 = bf16[12,4,1024]{2,1,0:T(4,128)(2,1)} copy(bf16[12,4,1024]{2,1,0:T(4,128)(2,1)} %shard_map.127) | data formatting | bytes 196608

commit v4 on v3

--- a/solution.py
+++ b/solution.py
@@ -14,6 +14,7 @@
 CORES = 2
 REACH = 4
 FIRST_BESIDE = 4
+FOLD = 4
 epsilon = 1e-06
 out_epsilon = 1e-10
 f32 = jnp.float32
@@ -82,7 +83,13 @@
     out_gain_ref,
     first_half,
     second_half,
+    strengths,
     spread,
+    tail_out,
+    tail_in,
+    select_buf,
+    owned_buf,
+    out_weights,
     rows_buf,
     conv_buf,
     maps,
@@ -95,6 +102,8 @@
     z_recv,
     y_send,
     y_recv,
+    g_send,
+    g_recv,
     q_send,
     q_recv,
     t_send,
@@ -119,7 +128,7 @@
     z, y = sp // seqs, sp % seqs
     x, core = tp // CORES, tp % CORES
     far = [hops // 2, (hops - 1) // 2]
-    halves = [first_half, second_half]
+    last = (y == seqs - 1) & (tp == group - 1)
     pending = []
 
     def at(dz, dy, dx, dc=0):
@@ -156,14 +165,14 @@
         pl.semaphore_signal(barrier, inc=1, device_id=device, device_id_type=MESH)
 
     def own(half, part):
-        return halves[half].at[z, y, :, pl.ds(part * depth, depth)]
+        return (first_half, second_half)[half].at[z, y, :, pl.ds(part * depth, depth)]
 
     loads = [
-        (tokens_hbm, tokens_ref),
-        (in_gain_hbm, in_gain_ref),
         (wk_hbm, own(0, 0)),
         (wv_hbm, own(0, 1)),
         (wb_hbm, beta_ref),
+        (tokens_hbm, tokens_ref),
+        (in_gain_hbm, in_gain_ref),
         (wq_hbm, own(1, 0)),
         (wg_hbm, own(1, 1)),
         (wo_hbm, own(1, 2)),
@@ -175,24 +184,44 @@
     loads = [pltpu.make_async_copy(a, b, load.at[i]) for i, (a, b) in enumerate(loads)]
     for one in loads:
         one.start()
+
+    full = PAD + span
+    padded = seqs * group * PAD
+    row, col = iota((full, padded), 0), iota((full, padded), 1)
+    place, inside = col // PAD, col % PAD
+    select = (row == PAD + place * here_rows + inside) & (inside < here_rows)
+    select = select | ((col - row == padded - PAD) & (inside >= here_rows) & (row < PAD))
+    select_buf[...] = jnp.where(select, 1.0, 0.0).astype(bf16)
+
+    order = [2, 1, 3, 0]
+    folded = FOLD * here_rows
+    batch = chips * folded
+    row = iota((batch, 1), 0).astype(f32) + 0.5
+    chip_of = jnp.floor(row / folded)
+    fold_of = jnp.floor(row / here_rows) - FOLD * chip_of
+    inside = row - 0.5 - here_rows * (FOLD * chip_of + fold_of)
+    first = (CORES * here_rows * chip_of + inside).astype(jnp.int32)
+    col = iota((batch, span), 1)
+    for cc in range(CORES):
+        for i, dy in enumerate(order):
+            begin = ((y + dy) % seqs * chips * CORES + cc) * here_rows
+            owned_buf[cc, i * batch : (i + 1) * batch, :] = jnp.where(
+                col == first + begin, 1.0, 0.0
+            ).astype(bf16)
+
     for one in loads:
         one.wait()
 
     block = wk_hbm.shape[0]
-    unit = jnp.where(iota((block, block), 0) == iota((block, block), 1), 1.0, 0.0)
-    column = jnp.broadcast_to(beta_ref[...].astype(f32), (depth, block))
-    first_half[z, y, :, 2 * depth :] = dot(unit, column, NT).astype(bf16)
-
-    pad_rows = jnp.zeros((PAD - here_rows, width), f32)
-    for seq in range(seqs):
-        values = tokens_ref[:, seq, :].astype(f32)
-        scaled = values * lax.rsqrt(jnp.mean(values * values, axis=-1, keepdims=True) + epsilon)
-        spread[seq] = jnp.concatenate([scaled * in_gain_ref[...], pad_rows], axis=0).astype(bf16)
+    strengths[z, y] = jnp.concatenate(
+        [beta_ref[...].astype(f32), jnp.zeros((1, depth - block), f32)], axis=1
+    )
 
     pl.semaphore_wait(barrier, len(friends))
 
     def z_copy(half, index, offset, device):
-        one = halves[half].at[(z + offset) % hops, y]
+        zz = (z + offset) % hops
+        one = strengths.at[zz] if half == 2 else (first_half, second_half)[half].at[zz, y]
         return copy(one, one, z_send.at[half, index], z_recv.at[half, index], device)
 
     def z_launch(half, index, offset, device):
@@ -237,10 +266,38 @@
             pending.append(one)
 
     def t_slot(yy, xx, cc):
-        return rows_buf.at[1 + (yy * chips + xx) * CORES + cc]
+        return rows_buf.at[(yy * chips + xx) * CORES + cc]
 
     relayed = far[0] > REACH
     z_first(0)
+    for dy in (2, 1, 3):
+        one = strengths.at[z, y]
+        launch(one, one, g_send.at[dy], g_recv.at[seqs - dy], at(0, dy, 0))
+    y_fan(0)
+
+    pad_rows = jnp.zeros((PAD - here_rows, width), f32)
+    tail_rows = PAD - here_rows
+    for seq in range(seqs):
+        values = tokens_ref[:, seq, :].astype(f32)
+        scaled = values * lax.rsqrt(jnp.mean(values * values, axis=-1, keepdims=True) + epsilon)
+        spread[seq] = jnp.concatenate([scaled * in_gain_ref[...], pad_rows], axis=0).astype(bf16)
+
+    tail = copy(tail_out, tail_in, h_send, h_recv, at(1, 0, 0))
+
+    @pl.when(last)
+    def _():
+        ends = [spread[seq].astype(f32)[here_rows - tail_rows : here_rows] for seq in range(seqs)]
+        tail_out[...] = jnp.concatenate(ends, axis=0).astype(bf16)
+        tail.start()
+        tail.wait_recv()
+        before = jnp.where(z > 0, tail_in[...].astype(f32), 0.0)
+        for seq in range(seqs):
+            rows = [
+                spread[seq].astype(f32)[:here_rows],
+                before[seq * tail_rows : (seq + 1) * tail_rows],
+            ]
+            spread[seq] = jnp.concatenate(rows, axis=0).astype(bf16)
+
     for index, (dy, dx) in enumerate(plane):
         launch(
             spread.at[(y + dy) % seqs],
@@ -249,9 +306,12 @@
             t_recv.at[(seqs - dy) % seqs * chips + (chips - dx) % chips],
             at(0, dy, dx),
         )
-    y_fan(0)
     launch(spread.at[y], t_slot(y, x, core), c_send.at[0], c_recv.at[0], partner)
-    rows_buf[1 + (y * chips + x) * CORES + core] = spread[y]
+    rows_buf[(y * chips + x) * CORES + core] = spread[y]
+    for dy in (1, 3, 2):
+        one = strengths.at[z, (y + dy) % seqs]
+        copy(one, one, g_send.at[dy], g_recv.at[dy], me).wait_recv()
+    z_first(2)
     z_first(1)
 
     if relayed:
@@ -269,39 +329,38 @@
         copy(slot, slot, t_send.at[0], t_recv.at[index], me).wait_recv()
         launch(slot, slot, c_send.at[index], c_recv.at[index], partner)
     if relayed:
+        z_relay(2)
         for d in range(REACH + 1, far[0] + 1):
             for index in [d, far[0] + d]:
                 if d <= far[index > far[0]]:
                     z_arrived(0, index)
                     y_fan(index)
         z_relay(1)
+    for d in range(1, far[0] + 1):
+        for index in [d, far[0] + d]:
+            if d <= far[index > far[0]] and not (relayed and d == REACH):
+                z_arrived(2, index)
     for dy, dx in [(0, 0)] + plane:
         index = dy * chips + dx
         slot = t_slot((y + dy) % seqs, (x + dx) % chips, (core + 1) % CORES)
         copy(slot, slot, c_send.at[0], c_recv.at[index], me).wait_recv()
-    history = copy(rows_buf.at[seqs * group], rows_buf.at[0], h_send, h_recv, at(1, 0, 0))
-    history.start()
-    pending.append(history)
     for index in range(far[0] + far[1] + 1):
         offset = offset_of(index) if index else 0
         for dy in (1, 3, 2):
             y_copy(index, dy, offset, (y + dy) % seqs, me).wait_recv()
-    history.wait_recv()
-
-    full = PAD + span
-    padded = (1 + seqs * group) * PAD
-    row, col = iota((full, padded), 0), iota((full, padded), 1)
-    place, inside = col // PAD, col % PAD
-    select = (row == PAD + (place - 1) * here_rows + inside) & (inside < here_rows)
-    select = jnp.where(select & ((place > 0) | (z > 0)), 1.0, 0.0).astype(bf16)
-
-    def project(half, columns):
-        weights = half[:, :, :, :columns].reshape(width, columns)
+
+    def project(weights):
         pre = dot(rows_buf[...].reshape(padded, width), weights).astype(bf16)
-        return dot(select, pre)
-
-    pre = project(first_half, 3 * depth)
-    conv_buf[:, : 2 * depth] = pre[:, : 2 * depth]
+        return dot(select_buf[...], pre)
+
+    devices = hops * seqs
+    pick = iota((width, devices), 0) // block == iota((width, devices), 1)
+    column = dot(jnp.where(pick, 1.0, 0.0), strengths[...].reshape(devices, depth))
+    column = jnp.where(iota((width, depth), 0) % block == iota((width, depth), 1), column, 0.0)
+    column = dot(column, jnp.ones((depth, depth), f32)).astype(bf16)
+    weights = first_half[...].reshape(width, 2 * depth)
+    pre = project(jnp.concatenate([weights, column], axis=1))
+    conv_buf[...] = pre[:, : 2 * depth]
     shift = math.log(depth / (4.0 * total_tokens))
     beta = jax.nn.sigmoid(pre[PAD:, 2 * depth :] + shift)
     width_taps = cq_ref.shape[0]
@@ -387,7 +446,10 @@
         for dy in (1, 3, 2):
             one = second_half.at[:, (y + dy) % seqs]
             copy(one, one, q_send.at[dy], q_recv.at[dy], me).wait_recv()
-        pre = project(second_half, 2 * depth)
+        pre = project(second_half[:, :, :, : 2 * depth].reshape(width, 2 * depth))
+        full_out = second_half[:, :, :, 2 * depth :].reshape(FOLD, width // FOLD, depth)
+        for fold in range(FOLD):
+            out_weights[:, fold * depth : (fold + 1) * depth] = full_out[fold]
         conv_buf[:, : depth] = pre[:, :depth]
         gate_pre = pre[PAD:, depth:]
         late_work["gate"] = gate_pre * jax.nn.sigmoid(gate_pre)
@@ -451,28 +513,22 @@
     out = out * lax.rsqrt(jnp.mean(out * out, axis=-1, keepdims=True) + out_epsilon)
     gated = (out * out_gain_ref[...] * late_work["gate"]).astype(bf16)
 
-    full_out = second_half[:, :, :, 2 * depth :].reshape(width, depth)
-    order = [2, 1, 3, 0]
-    batch = chips * PAD
-    row, col = iota((batch, span), 0), iota((batch, span), 1)
-
-    def owned_by(dy, cc):
-        owner = ((y + dy) % seqs * chips + row // PAD) * CORES + cc
-        match = (col == owner * here_rows + row % PAD) & (row % PAD < here_rows)
-        return jnp.where(match, 1.0, 0.0)
+    fold_row = fold_of.astype(jnp.int32)
 
     def products(cc):
-        rows = dot(jnp.concatenate([owned_by(dy, cc) for dy in order], axis=0), gated)
-        return dot(rows, full_out, NT)
+        rows = dot(owned_buf[cc], gated)
+        folds = jnp.concatenate([fold_row] * seqs, axis=0)
+        wide = [jnp.where(folds == fold, rows, 0.0).astype(bf16) for fold in range(FOLD)]
+        return dot(jnp.concatenate(wide, axis=1), out_weights[...], NT)
 
     theirs = products(1 - core).astype(bf16)
     for i in range(seqs):
-        swap_out[i] = theirs[i * batch : (i + 1) * batch].reshape(chips, PAD, width)
+        swap_out[i] = theirs[i * batch : (i + 1) * batch].reshape(chips, folded, -1)
         launch(swap_out.at[i], swap_in.at[i], s_send.at[i], s_recv.at[i], partner)
     mine = products(core)
     for i, dy in enumerate(order):
         copy(swap_in.at[i], swap_in.at[i], s_send.at[i], s_recv.at[i], me).wait_recv()
-        total = mine[i * batch : (i + 1) * batch].reshape(chips, PAD, width) + swap_in[i].astype(f32)
+        total = mine[i * batch : (i + 1) * batch].reshape(chips, folded, -1) + swap_in[i].astype(f32)
         parts[i] = total.astype(bf16)
         for dx in range(chips):
             if dy or dx:
@@ -492,9 +548,14 @@
         total = landed[seq * chips].astype(f32)
         for chip in range(1, chips):
             total = total + landed[seq * chips + chip].astype(f32)
-        out_ref[:, seq, :] = total[:here_rows].astype(bf16)
+        rows = [total[fold * here_rows : (fold + 1) * here_rows] for fold in range(FOLD)]
+        out_ref[:, seq, :] = jnp.concatenate(rows, axis=1).astype(bf16)
     for one in pending:
         one.wait_send()
+
+    @pl.when(last)
+    def _():
+        tail.wait_send()
 
 
 def body(
@@ -538,21 +599,29 @@
             vmem(conv_query.shape, bf16),
             vmem(conv_query.shape, bf16),
             vmem((1, depth), f32),
+            vmem((hops, seqs, block, 2 * depth), bf16),
             vmem((hops, seqs, block, 3 * depth), bf16),
-            vmem((hops, seqs, block, 3 * depth), bf16),
+            vmem((hops, seqs, 1, depth), f32),
             vmem((seqs, PAD, width), bf16),
-            vmem((1 + owners, PAD, width), bf16),
+            vmem((PAD, width), bf16),
+            vmem((PAD, width), bf16),
+            vmem((PAD + span, owners * PAD), bf16),
+            vmem((CORES, owners // CORES * FOLD * here_rows, span), bf16),
+            vmem((width // FOLD, FOLD * depth), bf16),
+            vmem((owners, PAD, width), bf16),
             vmem((PAD + span, 2 * depth), f32),
             vmem((hops, 2, depth, depth), bf16),
-            vmem((seqs, chips, PAD, width), bf16),
-            vmem((seqs, chips, PAD, width), bf16),
-            vmem((seqs, chips, PAD, width), bf16),
-            vmem((seqs * chips, PAD, width), bf16),
+            vmem((seqs, chips, FOLD * here_rows, width // FOLD), bf16),
+            vmem((seqs, chips, FOLD * here_rows, width // FOLD), bf16),
+            vmem((seqs, chips, FOLD * here_rows, width // FOLD), bf16),
+            vmem((seqs * chips, FOLD * here_rows, width // FOLD), bf16),
             dma((12,)),
-            dma((2, hops)),
-            dma((2, hops)),
+            dma((3, hops)),
+            dma((3, hops)),
             dma((hops, seqs)),
             dma((hops, seqs)),
+            dma((seqs,)),
+            dma((seqs,)),
             dma((seqs,)),
             dma((seqs,)),
             dma((seqs * chips,)),

time: 75 us -> 72 us (0.960)
  Pallas kernels: 72.6 us -> 69.6 us
    pallas_call x1, Pallas kernels: 72.6 us -> 69.6 us  [body(): pl.pallas_call(functools.partial(mixer_kernel, sizes), out_shape=jax.Shap...]
where the time goes in v4:
time: 72 us; the launch traced here: 71.8 us
  Pallas kernels  69.6 us (97%)
  local copies, waits for them, and re-layouts  1.57 us (2%)
    pallas_call x1, Pallas kernels, body(): pl.pallas_call(functools.partial(mixer_kernel, sizes), out_shape=jax.Shap...  69.6 us
    unnamed x1, local copies, waits for them, and re-layouts  1.57 us

profile of v4, /device:TPU:1, one launch (start us, length us, event | category | flops | bytes accessed | tf_op | source)
XLA Modules:
  0.0 71.8 jit_solution(15726669606149711672)
XLA Ops:
  0.7 69.6 %shard_map.127 = bf16[12,4,1024]{2,1,0:T(4,128)(2,1)} custom-call(bf16[12,4,1024]{2,1,0:T(4,128)(2,1)} %tokens_hbm.1, f32[1,1024]{1,0:T(1,128)} %bitcast.4, bf16[16,128]{1,0:T(8,128)(2,1)} %wq_hbm.1, bf16[16,128]{1,0:T(8,128)(2,1)} %wk_hbm.1, bf16[16,128]{1,0:T(8,128)(2,1)} %wv_hbm.1, bf16[16,128]{1,0:T(8,128)(2,1)} %wg_hbm.1, bf16[1,16]{1,0:T(2,128)(2,1)} %bitcast.6, ...), custom_call_target="tpu_custom_call" | custom-call | tf_op jit(solution)/shard_map/pallas_call | solution.py:589
  70.3 1.6 %copy.16 = bf16[12,4,1024]{2,1,0:T(4,128)(2,1)} copy(bf16[12,4,1024]{2,1,0:T(4,128)(2,1)} %shard_map.127) | data formatting | bytes 196608

commit v5 on v4

--- a/solution.py
+++ b/solution.py
@@ -89,6 +89,9 @@
     tail_in,
     select_buf,
     owned_buf,
+    reads_buf,
+    locals_buf,
+    gate_buf,
     out_weights,
     rows_buf,
     conv_buf,
@@ -168,11 +171,11 @@
         return (first_half, second_half)[half].at[z, y, :, pl.ds(part * depth, depth)]
 
     loads = [
+        (tokens_hbm, tokens_ref),
+        (in_gain_hbm, in_gain_ref),
         (wk_hbm, own(0, 0)),
         (wv_hbm, own(0, 1)),
         (wb_hbm, beta_ref),
-        (tokens_hbm, tokens_ref),
-        (in_gain_hbm, in_gain_ref),
         (wq_hbm, own(1, 0)),
         (wg_hbm, own(1, 1)),
         (wo_hbm, own(1, 2)),
@@ -185,31 +188,17 @@
     for one in loads:
         one.start()
 
-    full = PAD + span
-    padded = seqs * group * PAD
-    row, col = iota((full, padded), 0), iota((full, padded), 1)
-    place, inside = col // PAD, col % PAD
-    select = (row == PAD + place * here_rows + inside) & (inside < here_rows)
-    select = select | ((col - row == padded - PAD) & (inside >= here_rows) & (row < PAD))
-    select_buf[...] = jnp.where(select, 1.0, 0.0).astype(bf16)
-
-    order = [2, 1, 3, 0]
-    folded = FOLD * here_rows
-    batch = chips * folded
-    row = iota((batch, 1), 0).astype(f32) + 0.5
-    chip_of = jnp.floor(row / folded)
-    fold_of = jnp.floor(row / here_rows) - FOLD * chip_of
-    inside = row - 0.5 - here_rows * (FOLD * chip_of + fold_of)
-    first = (CORES * here_rows * chip_of + inside).astype(jnp.int32)
-    col = iota((batch, span), 1)
-    for cc in range(CORES):
-        for i, dy in enumerate(order):
-            begin = ((y + dy) % seqs * chips * CORES + cc) * here_rows
-            owned_buf[cc, i * batch : (i + 1) * batch, :] = jnp.where(
-                col == first + begin, 1.0, 0.0
-            ).astype(bf16)
-
-    for one in loads:
+    for one in loads[:2]:
+        one.wait()
+
+    pad_rows = jnp.zeros((PAD - here_rows, width), f32)
+    tail_rows = PAD - here_rows
+    for seq in range(seqs):
+        values = tokens_ref[:, seq, :].astype(f32)
+        scaled = values * lax.rsqrt(jnp.mean(values * values, axis=-1, keepdims=True) + epsilon)
+        spread[seq] = jnp.concatenate([scaled * in_gain_ref[...], pad_rows], axis=0).astype(bf16)
+
+    for one in loads[2:]:
         one.wait()
 
     block = wk_hbm.shape[0]
@@ -269,26 +258,72 @@
         return rows_buf.at[(yy * chips + xx) * CORES + cc]
 
     relayed = far[0] > REACH
+    tail = copy(tail_out, tail_in, h_send, h_recv, at(1, 0, 0))
+
+    @pl.when(last)
+    def _():
+        ends = [spread[seq].astype(f32)[here_rows - tail_rows : here_rows] for seq in range(seqs)]
+        tail_out[...] = jnp.concatenate(ends, axis=0).astype(bf16)
+        tail.start()
+
     z_first(0)
     for dy in (2, 1, 3):
         one = strengths.at[z, y]
         launch(one, one, g_send.at[dy], g_recv.at[seqs - dy], at(0, dy, 0))
     y_fan(0)
 
-    pad_rows = jnp.zeros((PAD - here_rows, width), f32)
-    tail_rows = PAD - here_rows
-    for seq in range(seqs):
-        values = tokens_ref[:, seq, :].astype(f32)
-        scaled = values * lax.rsqrt(jnp.mean(values * values, axis=-1, keepdims=True) + epsilon)
-        spread[seq] = jnp.concatenate([scaled * in_gain_ref[...], pad_rows], axis=0).astype(bf16)
-
-    tail = copy(tail_out, tail_in, h_send, h_recv, at(1, 0, 0))
+    token_copies = [
+        copy(
+            spread.at[(y + dy) % seqs],
+            t_slot(y, x, core),
+            t_send.at[dy * chips + dx],
+            t_recv.at[(seqs - dy) % seqs * chips + (chips - dx) % chips],
+            at(0, dy, dx),
+        )
+        for dy, dx in plane
+    ]
+    token_copies.append(
+        copy(spread.at[y], t_slot(y, x, core), c_send.at[0], c_recv.at[0], partner)
+    )
+    pending.extend(token_copies)
+
+    def send_tokens():
+        for one in token_copies:
+            one.start()
+        rows_buf[(y * chips + x) * CORES + core] = spread[y]
+
+    @pl.when(jnp.logical_not(last))
+    def _():
+        send_tokens()
+
+    full = PAD + span
+    padded = seqs * group * PAD
+    row, col = iota((full, padded), 0), iota((full, padded), 1)
+    place, inside = col // PAD, col % PAD
+    select = (row == PAD + place * here_rows + inside) & (inside < here_rows)
+    select = select | ((col - row == padded - PAD) & (inside >= here_rows) & (row < PAD))
+    select_buf[...] = jnp.where(select, 1.0, 0.0).astype(bf16)
+
+    order = [2, 1, 3, 0]
+    share = span // seqs
+    folded = FOLD * here_rows
+    batch = chips * folded
+    row = iota((batch, 1), 0).astype(f32) + 0.5
+    chip_of = jnp.floor(row / folded)
+    fold_of = jnp.floor(row / here_rows) - FOLD * chip_of
+    inside = row - 0.5 - here_rows * (FOLD * chip_of + fold_of)
+    first = (CORES * here_rows * chip_of + inside).astype(jnp.int32)
+    col = iota((batch, share), 1)
+    for cc in range(CORES):
+        owned_buf[cc] = jnp.where(col == first + cc * here_rows, 1.0, 0.0).astype(bf16)
+
+    for dy in (1, 3, 2):
+        one = strengths.at[z, (y + dy) % seqs]
+        copy(one, one, g_send.at[dy], g_recv.at[dy], me).wait_recv()
+    z_first(2)
 
     @pl.when(last)
     def _():
-        ends = [spread[seq].astype(f32)[here_rows - tail_rows : here_rows] for seq in range(seqs)]
-        tail_out[...] = jnp.concatenate(ends, axis=0).astype(bf16)
-        tail.start()
         tail.wait_recv()
         before = jnp.where(z > 0, tail_in[...].astype(f32), 0.0)
         for seq in range(seqs):
@@ -297,21 +332,8 @@
                 before[seq * tail_rows : (seq + 1) * tail_rows],
             ]
             spread[seq] = jnp.concatenate(rows, axis=0).astype(bf16)
-
-    for index, (dy, dx) in enumerate(plane):
-        launch(
-            spread.at[(y + dy) % seqs],
-            t_slot(y, x, core),
-            t_send.at[index],
-            t_recv.at[(seqs - dy) % seqs * chips + (chips - dx) % chips],
-            at(0, dy, dx),
-        )
-    launch(spread.at[y], t_slot(y, x, core), c_send.at[0], c_recv.at[0], partner)
-    rows_buf[(y * chips + x) * CORES + core] = spread[y]
-    for dy in (1, 3, 2):
-        one = strengths.at[z, (y + dy) % seqs]
-        copy(one, one, g_send.at[dy], g_recv.at[dy], me).wait_recv()
-    z_first(2)
+        send_tokens()
+
     z_first(1)
 
     if relayed:
@@ -323,11 +345,6 @@
             if d <= far[index > far[0]]:
                 z_arrived(0, index)
                 y_fan(index)
-    for dy, dx in plane:
-        index = dy * chips + dx
-        slot = t_slot((y + dy) % seqs, (x + dx) % chips, core)
-        copy(slot, slot, t_send.at[0], t_recv.at[index], me).wait_recv()
-        launch(slot, slot, c_send.at[index], c_recv.at[index], partner)
     if relayed:
         z_relay(2)
         for d in range(REACH + 1, far[0] + 1):
@@ -335,6 +352,12 @@
                 if d <= far[index > far[0]]:
                     z_arrived(0, index)
                     y_fan(index)
+    for dy, dx in plane:
+        index = dy * chips + dx
+        slot = t_slot((y + dy) % seqs, (x + dx) % chips, core)
+        copy(slot, slot, t_send.at[0], t_recv.at[index], me).wait_recv()
+        launch(slot, slot, c_send.at[index], c_recv.at[index], partner)
+    if relayed:
         z_relay(1)
     for d in range(1, far[0] + 1):
         for index in [d, far[0] + d]:
@@ -452,7 +475,7 @@
             out_weights[:, fold * depth : (fold + 1) * depth] = full_out[fold]
         conv_buf[:, : depth] = pre[:, :depth]
         gate_pre = pre[PAD:, depth:]
-        late_work["gate"] = gate_pre * jax.nn.sigmoid(gate_pre)
+        gate_buf[...] = out_gain_ref[...] * gate_pre * jax.nn.sigmoid(gate_pre)
 
     def queries_and_scores():
         queries = [
@@ -464,7 +487,6 @@
         ]
 
     def reads_and_locals():
-        reads, locals_ = [], []
         for chunk in range(CHUNKS):
             seen = dot(late_work["scores"][chunk], both[chunk])
             read = late_work["queries"][chunk] * kept - seen[:, depth:]
@@ -474,9 +496,9 @@
                 shifted = dot(read, jnp.concatenate([value, erase], axis=1))
                 local = local + shifted[:, :depth]
                 read = before_kept[chunk - 1] * read - shifted[:, depth:]
-            reads.append(read.astype(bf16))
-            locals_.append(local)
-        late_work["reads"], late_work["locals"] = reads, locals_
+            rows = slice(chunk * size, (chunk + 1) * size)
+            reads_buf[rows, :] = read.astype(bf16)
+            locals_buf[rows, :] = local
 
     beside = [project_second, queries_and_scores, reads_and_locals]
     stretch = running_kept
@@ -508,29 +530,28 @@
         one()
     state = late[0] + late_kept * early - dot(late[1], early)
 
-    out = jnp.concatenate(late_work["locals"], axis=0)
-    out = out + dot(jnp.concatenate(late_work["reads"], axis=0), state)
-    out = out * lax.rsqrt(jnp.mean(out * out, axis=-1, keepdims=True) + out_epsilon)
-    gated = (out * out_gain_ref[...] * late_work["gate"]).astype(bf16)
+    state = state.astype(bf16)
 
     fold_row = fold_of.astype(jnp.int32)
 
-    def products(cc):
-        rows = dot(owned_buf[cc], gated)
-        folds = jnp.concatenate([fold_row] * seqs, axis=0)
-        wide = [jnp.where(folds == fold, rows, 0.0).astype(bf16) for fold in range(FOLD)]
-        return dot(jnp.concatenate(wide, axis=1), out_weights[...], NT)
-
-    theirs = products(1 - core).astype(bf16)
-    for i in range(seqs):
-        swap_out[i] = theirs[i * batch : (i + 1) * batch].reshape(chips, folded, -1)
+    def products(rows_of, cc):
+        rows = dot(owned_buf[cc], rows_of)
+        wide = [jnp.where(fold_row == fold, rows, 0.0).astype(bf16) for fold in range(FOLD)]
+        return dot(jnp.concatenate(wide, axis=1), out_weights[...], NT).reshape(chips, folded, -1)
+
+    gated = []
+    for i, dy in enumerate(order):
+        rows = pl.ds(pl.multiple_of((y + dy) % seqs * share, PAD), share)
+        out = locals_buf[rows, :] + dot(reads_buf[rows, :], state)
+        out = out * lax.rsqrt(jnp.mean(out * out, axis=-1, keepdims=True) + out_epsilon)
+        gated.append((out * gate_buf[rows, :]).astype(bf16))
+        swap_out[i] = products(gated[i], 1 - core).astype(bf16)
         launch(swap_out.at[i], swap_in.at[i], s_send.at[i], s_recv.at[i], partner)
-    mine = products(core)
     for i, dy in enumerate(order):
+        mine = products(gated[i], core)
         copy(swap_in.at[i], swap_in.at[i], s_send.at[i], s_recv.at[i], me).wait_recv()
-        total = mine[i * batch : (i + 1) * batch].reshape(chips, folded, -1) + swap_in[i].astype(f32)
-        parts[i] = total.astype(bf16)
-        for dx in range(chips):
+        parts[i] = (mine + swap_in[i].astype(f32)).astype(bf16)
+        for dx in (2, 1, 3, 0) if chips == 4 else range(chips):
             if dy or dx:
                 launch(
                     parts.at[i, (x + dx) % chips],
@@ -606,7 +627,10 @@
             vmem((PAD, width), bf16),
             vmem((PAD, width), bf16),
             vmem((PAD + span, owners * PAD), bf16),
-            vmem((CORES, owners // CORES * FOLD * here_rows, span), bf16),
+            vmem((CORES, chips * FOLD * here_rows, span // seqs), bf16),
+            vmem((span, depth), bf16),
+            vmem((span, depth), f32),
+            vmem((span, depth), f32),
             vmem((width // FOLD, FOLD * depth), bf16),
             vmem((owners, PAD, width), bf16),
             vmem((PAD + span, 2 * depth), f32),

time: 72 us -> 70 us (0.972)
  Pallas kernels: 69.6 us -> 67.3 us
    pallas_call x1, Pallas kernels: 69.6 us -> 67.3 us  [body(): pl.pallas_call(functools.partial(mixer_kernel, sizes), out_shape=jax.Shap...]
where the time goes in v5:
time: 70 us; the launch traced here: 69.5 us
  Pallas kernels  67.3 us (96%)
  local copies, waits for them, and re-layouts  1.57 us (2%)
    pallas_call x1, Pallas kernels, body(): pl.pallas_call(functools.partial(mixer_kernel, sizes), out_shape=jax.Shap...  67.3 us
    unnamed x1, local copies, waits for them, and re-layouts  1.57 us

profile of v5, /device:TPU:1, one launch (start us, length us, event | category | flops | bytes accessed | tf_op | source)
XLA Modules:
  0.0 69.5 jit_solution(6394158540752683363)
XLA Ops:
  0.7 67.3 %shard_map.127 = bf16[12,4,1024]{2,1,0:T(4,128)(2,1)} custom-call(bf16[12,4,1024]{2,1,0:T(4,128)(2,1)} %tokens_hbm.1, f32[1,1024]{1,0:T(1,128)} %bitcast.4, bf16[16,128]{1,0:T(8,128)(2,1)} %wq_hbm.1, bf16[16,128]{1,0:T(8,128)(2,1)} %wk_hbm.1, bf16[16,128]{1,0:T(8,128)(2,1)} %wv_hbm.1, bf16[16,128]{1,0:T(8,128)(2,1)} %wg_hbm.1, bf16[1,16]{1,0:T(2,128)(2,1)} %bitcast.6, ...), custom_call_target="tpu_custom_call" | custom-call | tf_op jit(solution)/shard_map/pallas_call | solution.py:610
  67.9 1.6 %copy.16 = bf16[12,4,1024]{2,1,0:T(4,128)(2,1)} copy(bf16[12,4,1024]{2,1,0:T(4,128)(2,1)} %shard_map.127) | data formatting | bytes 196608

commit v6 on v5

--- a/solution.py
+++ b/solution.py
@@ -437,21 +437,46 @@
         one = maps.at[source[side](offset), part]
         return copy(one, one, m_send.at[side, hop, part], m_recv.at[side, hop, part], device)
 
+    guarded = []
+
+    def useful(side, behind, step):
+        if side == 0:
+            return (z >= behind) & (z + step < hops)
+        first = (z + behind) % hops
+        if step == 2:
+            return first < far[1]
+        return (first < far[1]) & (first < behind + step)
+
     def m_forward(behind):
         for step in (2, 1):
-            for part in range(2):
-                for side in range(2):
-                    if behind + step <= far[side]:
-                        device = at(step if side == 0 else hops - step, 0, 0)
-                        one = m_copy(side, behind + step, part, behind, device)
-                        one.start()
-                        pending.append(one)
+            for side in range(2):
+                if behind + step <= far[side]:
+                    device = at(step if side == 0 else hops - step, 0, 0)
+                    both_parts = [
+                        m_copy(side, behind + step, part, behind, device) for part in range(2)
+                    ]
+                    needed = useful(side, behind, step)
+                    guarded.append((needed, both_parts))
+
+                    @pl.when(needed)
+                    def _():
+                        for one in both_parts:
+                            one.start()
 
     def m_arrived(hop):
-        for part in range(2):
-            for side in range(2):
-                if hop <= far[side]:
-                    m_copy(side, hop, part, hop, me).wait_recv()
+        for side in range(2):
+            if hop <= far[side]:
+                first = (z + hop) % hops
+                needed = z >= hop
+                if side == 1:
+                    needed = first < far[1]
+                    if hop % 2:
+                        needed = needed & (first < hop)
+
+                @pl.when(needed)
+                def _():
+                    for part in range(2):
+                        m_copy(side, hop, part, hop, me).wait_recv()
 
     m_forward(0)
 
@@ -514,7 +539,7 @@
                 m_arrived(hop)
             zz = source[0](hop)
             value = jnp.where(z >= hop, maps[zz, 0].astype(f32), 0.0)
-            erase = maps[zz, 1].astype(f32)
+            erase = jnp.where(z >= hop, maps[zz, 1].astype(f32), 0.0)
             if late is None:
                 late, late_kept = (value, erase), stretch
             else:
@@ -573,6 +598,13 @@
         out_ref[:, seq, :] = jnp.concatenate(rows, axis=1).astype(bf16)
     for one in pending:
         one.wait_send()
+
+    for needed, both_parts in guarded:
+
+        @pl.when(needed)
+        def _():
+            for one in both_parts:
+                one.wait_send()
 
     @pl.when(last)
     def _():

time: 70 us -> 63 us (0.900)
  Pallas kernels: 67.3 us -> 60.1 us
    pallas_call x1, Pallas kernels: 67.3 us -> 60.1 us  [body(): pl.pallas_call(functools.partial(mixer_kernel, sizes), out_shape=jax.Shap...]
where the time goes in v6:
time: 63 us; the launch traced here: 62.3 us
  Pallas kernels  60.1 us (95%)
  local copies, waits for them, and re-layouts  1.57 us (2%)
  between operations  0.66 us (1%)
    pallas_call x1, Pallas kernels, body(): pl.pallas_call(functools.partial(mixer_kernel, sizes), out_shape=jax.Shap...  60.1 us
    unnamed x1, local copies, waits for them, and re-layouts  1.57 us

profile of v6, /device:TPU:1, one launch (start us, length us, event | category | flops | bytes accessed | tf_op | source)
XLA Modules:
  0.0 62.3 jit_solution(4083992434630752375)
XLA Ops:
  0.7 60.1 %shard_map.127 = bf16[12,4,1024]{2,1,0:T(4,128)(2,1)} custom-call(bf16[12,4,1024]{2,1,0:T(4,128)(2,1)} %tokens_hbm.1, f32[1,1024]{1,0:T(1,128)} %bitcast.4, bf16[16,128]{1,0:T(8,128)(2,1)} %wq_hbm.1, bf16[16,128]{1,0:T(8,128)(2,1)} %wk_hbm.1, bf16[16,128]{1,0:T(8,128)(2,1)} %wv_hbm.1, bf16[16,128]{1,0:T(8,128)(2,1)} %wg_hbm.1, bf16[1,16]{1,0:T(2,128)(2,1)} %bitcast.6, ...), custom_call_target="tpu_custom_call" | custom-call | tf_op jit(solution)/shard_map/pallas_call | solution.py:642
  60.8 1.6 %copy.16 = bf16[12,4,1024]{2,1,0:T(4,128)(2,1)} copy(bf16[12,4,1024]{2,1,0:T(4,128)(2,1)} %shard_map.127) | data formatting | bytes 196608

commit v7 on v5

--- a/solution.py
+++ b/solution.py
@@ -15,6 +15,7 @@
 REACH = 4
 FIRST_BESIDE = 4
 FOLD = 4
+PIECES = 2
 epsilon = 1e-06
 out_epsilon = 1e-10
 f32 = jnp.float32
@@ -92,6 +93,8 @@
     reads_buf,
     locals_buf,
     gate_buf,
+    column_buf,
+    beta_buf,
     out_weights,
     rows_buf,
     conv_buf,
@@ -363,29 +366,30 @@
         for index in [d, far[0] + d]:
             if d <= far[index > far[0]] and not (relayed and d == REACH):
                 z_arrived(2, index)
+    devices = hops * seqs
+    pick = iota((width, devices), 0) // block == iota((width, devices), 1)
+    column = dot(jnp.where(pick, 1.0, 0.0), strengths[...].reshape(devices, depth))
+    column = jnp.where(iota((width, depth), 0) % block == iota((width, depth), 1), column, 0.0)
+    column_buf[...] = dot(column, jnp.ones((depth, depth), f32)).astype(bf16)
+
     for dy, dx in [(0, 0)] + plane:
         index = dy * chips + dx
         slot = t_slot((y + dy) % seqs, (x + dx) % chips, (core + 1) % CORES)
         copy(slot, slot, c_send.at[0], c_recv.at[index], me).wait_recv()
+    def project(weights):
+        pre = dot(rows_buf[...].reshape(padded, width), weights).astype(bf16)
+        return dot(select_buf[...], pre)
+
+    shift = math.log(depth / (4.0 * total_tokens))
+    beta_buf[...] = jax.nn.sigmoid(project(column_buf[...])[PAD:] + shift)
+
     for index in range(far[0] + far[1] + 1):
         offset = offset_of(index) if index else 0
         for dy in (1, 3, 2):
             y_copy(index, dy, offset, (y + dy) % seqs, me).wait_recv()
 
-    def project(weights):
-        pre = dot(rows_buf[...].reshape(padded, width), weights).astype(bf16)
-        return dot(select_buf[...], pre)
-
-    devices = hops * seqs
-    pick = iota((width, devices), 0) // block == iota((width, devices), 1)
-    column = dot(jnp.where(pick, 1.0, 0.0), strengths[...].reshape(devices, depth))
-    column = jnp.where(iota((width, depth), 0) % block == iota((width, depth), 1), column, 0.0)
-    column = dot(column, jnp.ones((depth, depth), f32)).astype(bf16)
-    weights = first_half[...].reshape(width, 2 * depth)
-    pre = project(jnp.concatenate([weights, column], axis=1))
-    conv_buf[...] = pre[:, : 2 * depth]
-    shift = math.log(depth / (4.0 * total_tokens))
-    beta = jax.nn.sigmoid(pre[PAD:, 2 * depth :] + shift)
+    pre = project(first_half[...].reshape(width, 2 * depth))
+    conv_buf[...] = pre
     width_taps = cq_ref.shape[0]
 
     def conv(part, taps_ref, begin):
@@ -408,7 +412,7 @@
         begin = chunk * size
         keys.append(l2_normalize(conv(0, ck_ref, begin)))
         values.append(conv(1, cv_ref, begin))
-        betas.append(beta[begin : begin + size])
+        betas.append(beta_buf[begin : begin + size, :])
     weighted = [k * b for k, b in zip(keys, betas)]
     lowers = [
         jnp.where(row > col, dot(w, k, NT) * decay, 0.0) for w, k in zip(weighted, keys)
@@ -433,32 +437,58 @@
 
     source = [lambda d: (z + hops - d) % hops, lambda d: (z + d) % hops]
 
-    def m_copy(side, hop, part, offset, device):
-        one = maps.at[source[side](offset), part]
-        return copy(one, one, m_send.at[side, hop, part], m_recv.at[side, hop, part], device)
-
-    def m_forward(behind):
-        for step in (2, 1):
-            for part in range(2):
-                for side in range(2):
-                    if behind + step <= far[side]:
-                        device = at(step if side == 0 else hops - step, 0, 0)
-                        one = m_copy(side, behind + step, part, behind, device)
-                        one.start()
-                        pending.append(one)
-
-    def m_arrived(hop):
-        for part in range(2):
+    def m_copy(side, hop, piece, offset, device):
+        rows = depth * 2 // PIECES
+        part, begin = piece * rows // depth, piece * rows % depth
+        one = maps.at[source[side](offset), part, pl.ds(begin, rows)]
+        return copy(one, one, m_send.at[side, hop, piece], m_recv.at[side, hop, piece], device)
+
+    guarded = []
+
+    def useful(side, behind, step):
+        if side == 0:
+            return (z >= behind) & (z + step < hops)
+        first = (z + behind) % hops
+        if step == 2:
+            return first < far[1]
+        return (first < far[1]) & (first < behind + step)
+
+    def m_forward(side, behind, step, piece):
+        if behind + step <= far[side]:
+            device = at(step if side == 0 else hops - step, 0, 0)
+            one = m_copy(side, behind + step, piece, behind, device)
+            needed = useful(side, behind, step)
+            guarded.append((needed, one))
+            pl.when(needed)(one.start)
+
+    def m_arrived(side, hop, piece):
+        if hop <= far[side]:
+            first = (z + hop) % hops
+            needed = z >= hop
+            if side == 1:
+                needed = first < far[1]
+                if hop % 2:
+                    needed = needed & (first < hop)
+            pl.when(needed)(m_copy(side, hop, piece, hop, me).wait_recv)
+
+    def m_stage(behind):
+        for piece in range(PIECES):
             for side in range(2):
-                if hop <= far[side]:
-                    m_copy(side, hop, part, hop, me).wait_recv()
-
-    m_forward(0)
+                if behind:
+                    m_arrived(side, behind, piece)
+                m_forward(side, behind, 2, piece)
+        for piece in range(PIECES):
+            for side in range(2):
+                m_forward(side, behind, 1, piece)
+
+    m_stage(0)
 
     for d in range(1, far[0] + 1):
         for index in [d, far[0] + d]:
             if d <= far[index > far[0]] and not (relayed and d == REACH):
                 z_arrived(1, index)
+    finished = list(pending)
+    pending.clear()
     for dy in (2, 1, 3):
         one = second_half.at[:, y]
         launch(one, one, q_send.at[dy], q_recv.at[seqs - dy], at(0, dy, 0))
@@ -504,17 +534,18 @@
     stretch = running_kept
     late, late_kept, early = None, None, jnp.zeros((depth, depth), f32)
     for stage in range(2, far[0] + 2, 2):
-        if stage <= far[0]:
-            m_arrived(stage)
-            m_forward(stage)
+        if stage < far[0]:
+            m_stage(stage)
         for hop in (stage - 1, stage):
             if hop > far[0]:
                 continue
-            if hop < stage:
-                m_arrived(hop)
+            if hop < stage or stage >= far[0]:
+                for piece in range(PIECES):
+                    for side in range(2):
+                        m_arrived(side, hop, piece)
             zz = source[0](hop)
             value = jnp.where(z >= hop, maps[zz, 0].astype(f32), 0.0)
-            erase = maps[zz, 1].astype(f32)
+            erase = jnp.where(z >= hop, maps[zz, 1].astype(f32), 0.0)
             if late is None:
                 late, late_kept = (value, erase), stretch
             else:
@@ -524,8 +555,12 @@
                 zz = source[1](hop)
                 new = stretch * early + maps[zz, 0].astype(f32) - dot(maps[zz, 1], early)
                 early = jnp.where(z + hop >= hops, new, 0.0)
-        if stage >= FIRST_BESIDE and beside:
-            beside.pop(0)()
+        if stage == FIRST_BESIDE:
+            for one in finished:
+                one.wait_send()
+        if stage >= FIRST_BESIDE:
+            for _ in range(min(len(beside), 1 if stage == FIRST_BESIDE else 2)):
+                beside.pop(0)()
     for one in beside:
         one()
     state = late[0] + late_kept * early - dot(late[1], early)
@@ -573,6 +608,9 @@
         out_ref[:, seq, :] = jnp.concatenate(rows, axis=1).astype(bf16)
     for one in pending:
         one.wait_send()
+
+    for needed, one in guarded:
+        pl.when(needed)(one.wait_send)
 
     @pl.when(last)
     def _():
@@ -631,6 +669,8 @@
             vmem((span, depth), bf16),
             vmem((span, depth), f32),
             vmem((span, depth), f32),
+            vmem((width, depth), bf16),
+            vmem((span, depth), f32),
             vmem((width // FOLD, FOLD * depth), bf16),
             vmem((owners, PAD, width), bf16),
             vmem((PAD + span, 2 * depth), f32),
@@ -654,8 +694,8 @@
             dma((seqs * chips,)),
             dma,
             dma,
-            dma((2, far, 2)),
-            dma((2, far, 2)),
+            dma((2, far, PIECES)),
+            dma((2, far, PIECES)),
             dma((seqs,)),
             dma((seqs,)),
             dma((seqs * chips,)),

time: 70 us -> 62.3 us (0.89)
  Pallas kernels: 67.3 us -> 59.3 us
    pallas_call x1, Pallas kernels: 67.3 us -> 59.3 us  [body(): pl.pallas_call(functools.partial(mixer_kernel, sizes), out_shape=jax.Shap...]
where the time goes in v7:
time: 62.3 us; the launch traced here: 61.6 us
  Pallas kernels  59.3 us (95%)
  local copies, waits for them, and re-layouts  1.57 us (3%)
  between operations  0.66 us (1%)
    pallas_call x1, Pallas kernels, body(): pl.pallas_call(functools.partial(mixer_kernel, sizes), out_shape=jax.Shap...  59.3 us
    unnamed x1, local copies, waits for them, and re-layouts  1.57 us

profile of v7, /device:TPU:1, one launch (start us, length us, event | category | flops | bytes accessed | tf_op | source)
XLA Modules:
  0.0 61.6 jit_solution(11345373580163059304)
XLA Ops:
  0.7 59.3 %shard_map.127 = bf16[12,4,1024]{2,1,0:T(4,128)(2,1)} custom-call(bf16[12,4,1024]{2,1,0:T(4,128)(2,1)} %tokens_hbm.1, f32[1,1024]{1,0:T(1,128)} %bitcast.4, bf16[16,128]{1,0:T(8,128)(2,1)} %wq_hbm.1, bf16[16,128]{1,0:T(8,128)(2,1)} %wk_hbm.1, bf16[16,128]{1,0:T(8,128)(2,1)} %wv_hbm.1, bf16[16,128]{1,0:T(8,128)(2,1)} %wg_hbm.1, bf16[1,16]{1,0:T(2,128)(2,1)} %bitcast.6, ...), custom_call_target="tpu_custom_call" | custom-call | tf_op jit(solution)/shard_map/pallas_call | solution.py:648
  60.0 1.6 %copy.16 = bf16[12,4,1024]{2,1,0:T(4,128)(2,1)} copy(bf16[12,4,1024]{2,1,0:T(4,128)(2,1)} %shard_map.127) | data formatting | bytes 196608

commit v8 on v7

--- a/solution.py
+++ b/solution.py
@@ -273,8 +273,6 @@
     for dy in (2, 1, 3):
         one = strengths.at[z, y]
         launch(one, one, g_send.at[dy], g_recv.at[seqs - dy], at(0, dy, 0))
-    y_fan(0)
-
     token_copies = [
         copy(
             spread.at[(y + dy) % seqs],
@@ -298,6 +296,8 @@
     @pl.when(jnp.logical_not(last))
     def _():
         send_tokens()
+
+    y_fan(0)
 
     full = PAD + span
     padded = seqs * group * PAD
@@ -355,7 +355,7 @@
                 if d <= far[index > far[0]]:
                     z_arrived(0, index)
                     y_fan(index)
-    for dy, dx in plane:
+    for dy, dx in sorted(plane, key=lambda p: min(p[0], seqs - p[0]) + min(p[1], chips - p[1])):
         index = dy * chips + dx
         slot = t_slot((y + dy) % seqs, (x + dx) % chips, core)
         copy(slot, slot, t_send.at[0], t_recv.at[index], me).wait_recv()

time: 62.3 us -> 61.8 us (level)
  no operation moved by 1% of the time
where the time goes in v8:
time: 61.8 us; the launch traced here: 61 us
  Pallas kernels  58.8 us (95%)
  local copies, waits for them, and re-layouts  1.57 us (3%)
  between operations  0.66 us (1%)
    pallas_call x1, Pallas kernels, body(): pl.pallas_call(functools.partial(mixer_kernel, sizes), out_shape=jax.Shap...  58.8 us
    unnamed x1, local copies, waits for them, and re-layouts  1.57 us

profile of v8, /device:TPU:1, one launch (start us, length us, event | category | flops | bytes accessed | tf_op | source)
XLA Modules:
  0.0 61.0 jit_solution(4158801355720047173)
XLA Ops:
  0.7 58.8 %shard_map.127 = bf16[12,4,1024]{2,1,0:T(4,128)(2,1)} custom-call(bf16[12,4,1024]{2,1,0:T(4,128)(2,1)} %tokens_hbm.1, f32[1,1024]{1,0:T(1,128)} %bitcast.4, bf16[16,128]{1,0:T(8,128)(2,1)} %wq_hbm.1, bf16[16,128]{1,0:T(8,128)(2,1)} %wk_hbm.1, bf16[16,128]{1,0:T(8,128)(2,1)} %wv_hbm.1, bf16[16,128]{1,0:T(8,128)(2,1)} %wg_hbm.1, bf16[1,16]{1,0:T(2,128)(2,1)} %bitcast.6, ...), custom_call_target="tpu_custom_call" | custom-call | tf_op jit(solution)/shard_map/pallas_call | solution.py:648
  59.4 1.6 %copy.16 = bf16[12,4,1024]{2,1,0:T(4,128)(2,1)} copy(bf16[12,4,1024]{2,1,0:T(4,128)(2,1)} %shard_map.127) | data formatting | bytes 196608

commit v9 on v8

--- a/solution.py
+++ b/solution.py
@@ -10,7 +10,7 @@
 
 MESH = pl.DeviceIdType.MESH
 PAD = 16
-CHUNKS = 3
+CHUNKS = 4
 CORES = 2
 REACH = 4
 FIRST_BESIDE = 4
@@ -425,13 +425,11 @@
     moved = [dot(k * rest, b, TN) for k, b in zip(keys, both)]
     chunk_maps = [(m[:, :depth], m[:, depth:]) for m in moved]
     chunk_kept = jnp.exp(-rate * jnp.full((1, depth), float(size), f32))
-    before, before_kept = [], []
-    running, running_kept = chunk_maps[0], chunk_kept
-    for chunk in range(1, CHUNKS):
-        before.append(running)
-        before_kept.append(running_kept)
-        running = compose(running, running_kept, chunk_maps[chunk], chunk_kept)
-        running_kept = running_kept * chunk_kept
+    kept_two = chunk_kept * chunk_kept
+    front = compose(chunk_maps[0], chunk_kept, chunk_maps[1], chunk_kept)
+    back = compose(chunk_maps[2], chunk_kept, chunk_maps[3], chunk_kept)
+    running = compose(front, kept_two, back, kept_two)
+    running_kept = kept_two * kept_two
     for part in range(2):
         maps[z, part] = running[part].astype(bf16)
 
@@ -482,6 +480,9 @@
                 m_forward(side, behind, 1, piece)
 
     m_stage(0)
+    third = compose(front, kept_two, chunk_maps[2], chunk_kept)
+    before = [chunk_maps[0], front, third]
+    before_kept = [chunk_kept, kept_two, kept_two * chunk_kept]
 
     for d in range(1, far[0] + 1):
         for index in [d, far[0] + d]:

time: 61.8 us -> 61.7 us (level)
  no operation moved by 1% of the time
where the time goes in v9:
time: 61.7 us; the launch traced here: 60.8 us
  Pallas kernels  58.6 us (95%)
  local copies, waits for them, and re-layouts  1.57 us (3%)
  between operations  0.66 us (1%)
    pallas_call x1, Pallas kernels, body(): pl.pallas_call(functools.partial(mixer_kernel, sizes), out_shape=jax.Shap...  58.6 us
    unnamed x1, local copies, waits for them, and re-layouts  1.57 us

profile of v9, /device:TPU:1, one launch (start us, length us, event | category | flops | bytes accessed | tf_op | source)
XLA Modules:
  0.0 60.8 jit_solution(14289329539005879051)
XLA Ops:
  0.7 58.6 %shard_map.127 = bf16[12,4,1024]{2,1,0:T(4,128)(2,1)} custom-call(bf16[12,4,1024]{2,1,0:T(4,128)(2,1)} %tokens_hbm.1, f32[1,1024]{1,0:T(1,128)} %bitcast.4, bf16[16,128]{1,0:T(8,128)(2,1)} %wq_hbm.1, bf16[16,128]{1,0:T(8,128)(2,1)} %wk_hbm.1, bf16[16,128]{1,0:T(8,128)(2,1)} %wv_hbm.1, bf16[16,128]{1,0:T(8,128)(2,1)} %wg_hbm.1, bf16[1,16]{1,0:T(2,128)(2,1)} %bitcast.6, ...), custom_call_target="tpu_custom_call" | custom-call | tf_op jit(solution)/shard_map/pallas_call | solution.py:649
  59.3 1.6 %copy.16 = bf16[12,4,1024]{2,1,0:T(4,128)(2,1)} copy(bf16[12,4,1024]{2,1,0:T(4,128)(2,1)} %shard_map.127) | data formatting | bytes 196608
